TPU v7x, 512 devices: a whole 4x4x16 slice. The times are simulated.
512 devices in a mesh: ep: 32 (over z, core), tp: 16 (over y, x).
Axes of the slice: x: 4, y: 4, z: 16, core: 2. Of those that a mesh axis runs over, the one named last changes fastest.
Arguments:
- tokens: bfloat16 [4096, 1024], P('ep', 'tp'), may hold values from -6 to 6
- norm_gain: float32 [1024], replicated, may hold values from 0.1 to 1.9
- gate_weight: bfloat16 [32, 1024, 1024], P('ep', None, 'tp'), may hold values from -0.1875 to 0.1875
- up_weight: bfloat16 [32, 1024, 1024], P('ep', None, 'tp'), may hold values from -0.1875 to 0.1875
- down_weight: bfloat16 [32, 1024, 1024], P('ep', None, 'tp'), may hold values from -0.1875 to 0.1875
- expert_ids: int32 [4096, 4], P('ep'), may hold values from 0 to 31, all different within a row; in each aligned block of 128 rows (0 to 127, 128 to 255, ...) at most 32 rows name the same one
- route_weight: float32 [4096, 4], P('ep'), may hold values from 0.2 to 1
Outputs:
- combined: bfloat16 [4096, 1024], P('ep', 'tp')
Inputs may be any that keep to these rules, and one draw needn't show every extreme that they name: `expert_ids`: each token names 4 different experts; in each aligned block of 128 tokens no expert is named by more than 32 of them, and in some block one expert is named by exactly 32; every expert is named by some token.
All inputs are finite; a program needn't handle non-finite values.
Results may differ from a plain program's by a relative error of at most 0.0035.
Values may be sent and summed in bfloat16 or wider, within the bound.
No kernel may reach another device: no remote copies, remote signals or barrier semaphores. Data moves between devices by JAX's collectives and lax.ppermute only.
A program may use at most 64 MiB of HBM per device.

v0:
```python
import functools

import jax
import jax.numpy as jnp
from jax import lax
from jax.experimental import pallas as pl
from jax.experimental.pallas import tpu as pltpu
from jax.sharding import Mesh
from jax.sharding import PartitionSpec as P


Z, CORE, TY, TX = "z", "core", "ty", "tx"
EP, TP = (Z, CORE), (TY, TX)
EPSILON = 1e-06
ALPHA = 1.702
LIMIT = 7.0
BF16, F32, I32 = jnp.bfloat16, jnp.float32, jnp.int32
NT = (((1,), (1,)), ((), ()))


def iota(shape, dim):
    return lax.broadcasted_iota(I32, shape, dim)


def dot(a, b):
    return jnp.dot(a, b, preferred_element_type=F32)


def dot_nt(a, b):
    return lax.dot_general(a, b, NT, preferred_element_type=F32)


def ones_where(mask):
    return jnp.where(mask, 1.0, 0.0).astype(BF16)


def moved(rows, sizes, order):
    count = rows.shape[0]
    left, source = iota((count, 1), 0), jnp.zeros((count, 1), I32)
    for axis in reversed(order):
        stride = 1
        for size in sizes[axis + 1 :]:
            stride *= size
        source = source + (left & (sizes[axis] - 1)) * stride
        left = left >> (sizes[axis].bit_length() - 1)
    select = ones_where(iota((count, count), 1) == source)
    return dot(select, rows).astype(BF16)


def halves(first, second):
    wide = first.shape[1] // 2
    left = iota(first.shape, 1) < wide
    return (
        jnp.where(left, first, pltpu.roll(second, wide, 1)),
        jnp.where(left, pltpu.roll(first, wide, 1), second),
    )


def prep_kernel(
    sizes, ids_hbm, tokens_hbm, gate_hbm, up_hbm, down_hbm, sent_ref, place_ref, shard_ref,
    ids_ref, tokens_ref, sems
):
    nz, cores, nx = sizes
    small = [(ids_hbm, ids_ref), (tokens_hbm, tokens_ref)]
    large = [(w, shard_ref.at[i]) for i, w in enumerate((gate_hbm, up_hbm, down_hbm))]
    copies = [pltpu.make_async_copy(a, b, sems.at[i]) for i, (a, b) in enumerate(small + large)]
    for copy in copies:
        copy.start()
    top, toks = ids_ref.shape
    count, _ = sent_ref.shape
    experts = nz * cores
    half = count // experts
    inner = half // nx
    earlier = ones_where(iota((toks, toks), 0) < iota((toks, toks), 1))
    expert = iota((experts, toks), 0)
    copies[0].wait()
    ids = ids_ref[...]
    picks = [expert == ids[k : k + 1] for k in range(top)]
    named = picks[0]
    for pick in picks[1:]:
        named = named | pick
    before = dot(ones_where(named), earlier)
    lane = iota((2 * count, toks), 0)
    hit = None
    for k in range(top):
        slot = jnp.sum(jnp.where(picks[k], before, 0.0), axis=0, keepdims=True).astype(I32)
        low, high = slot & (half - 1), jnp.where(slot >= half, count, 0)
        owner = ids[k : k + 1]
        place_ref[k : k + 1] = owner * half + low + high
        x, r = low >> (inner.bit_length() - 1), low & (inner - 1)
        z, core = owner >> (cores.bit_length() - 1), owner & (cores - 1)
        place = ((z * nx + x) * cores + core) * inner + r + high
        hit = (lane == place) if hit is None else hit | (lane == place)
    select = ones_where(hit)
    copies[1].wait()
    tokens = tokens_ref[...].astype(F32)
    zero = jnp.zeros_like(tokens)
    both = jnp.concatenate(
        [jnp.concatenate([tokens, zero], 1), jnp.concatenate([zero, tokens], 1)], 0
    ).astype(BF16)
    both_select = jnp.concatenate([select[:count], select[count:]], 1)
    sent_ref[...] = dot_nt(both_select, both).astype(BF16)
    for copy in copies[2:]:
        copy.wait()


def mix_kernel(place_ref, weight_ref, first_ref, rest_ref):
    count, toks = first_ref.shape
    lane = iota((count, toks), 0)
    mix = jnp.zeros((count, toks), F32)
    for k in range(place_ref.shape[0]):
        mix = mix + jnp.where(lane == place_ref[k : k + 1], weight_ref[k : k + 1], 0.0)
    first = mix.astype(BF16)
    first_ref[...] = first
    rest_ref[...] = (mix - first.astype(F32)).astype(BF16)


def spread_kernel(sizes, got_ref, out_ref):
    cores, copies, _, _, _ = out_ref.shape
    rows = moved(got_ref[...], sizes, (2, 1, 0, 3)).reshape((cores,) + out_ref.shape[2:])
    for core in range(cores):
        for c in range(copies):
            out_ref[core, c] = rows[core]


def up_kernel(rows_ref, gain_ref, weights_ref, out_ref, whole, normed):
    cores, pieces, part, wide = rows_ref.shape
    group = cores * part
    full = normed.shape[1]
    squares = [jnp.zeros((group, wide), F32) for _ in range(2)]
    for j in range(pieces // 2):
        even, odd = (
            jnp.concatenate([rows_ref[c, 2 * j + i].astype(F32) for c in range(cores)], 0)
            for i in range(2)
        )
        pair = halves(even, odd)
        for h in range(2):
            whole[h * group : (h + 1) * group, j * wide : (j + 1) * wide] = pair[h]
            squares[h] = squares[h] + pair[h] * pair[h]
    for h in range(2):
        mean = jnp.sum(squares[h], axis=1, keepdims=True) / full
        inverse = lax.rsqrt(mean + EPSILON)
        rows = slice(h * group, (h + 1) * group)
        normed[rows] = (whole[rows] * inverse * gain_ref[...]).astype(BF16)
    nx, _, units, _ = weights_ref.shape
    w_gate = weights_ref[:, 0].reshape(nx * units, full)
    w_up = weights_ref[:, 1].reshape(nx * units, full)
    gate = jnp.minimum(dot_nt(normed[...], w_gate), LIMIT)
    up = jnp.clip(dot_nt(normed[...], w_up), -LIMIT, LIMIT)
    hidden = ((up + 1.0) * gate * jax.nn.sigmoid(ALPHA * gate)).astype(BF16)
    for c in range(out_ref.shape[0]):
        out_ref[c] = hidden


def down_kernel(sizes, hidden_ref, weights_ref, out_ref):
    ny, rows, units = hidden_ref.shape
    nx, _, width, full = weights_ref.shape
    w_down = weights_ref[:, 2].reshape(nx * width, full)
    total = dot_nt(hidden_ref[0], w_down[:, :units])
    for y in range(1, ny):
        total = total + dot_nt(hidden_ref[y], w_down[:, y * units : (y + 1) * units])
    group = rows // 2
    pieces = []
    for j in range(nx // 2):
        lanes = slice(2 * j * width, 2 * (j + 1) * width)
        pieces += halves(total[:group, lanes], total[group:, lanes])
    stacked = jnp.concatenate(pieces, 0).astype(BF16)
    out_ref[...] = moved(stacked, sizes, (2, 1, 0, 3))


def combine_kernel(back_ref, first_ref, rest_ref, out_ref):
    count = back_ref.shape[0]
    width = out_ref.shape[0]
    back = back_ref[...].astype(F32).T.astype(BF16)
    total = jnp.zeros(out_ref.shape, F32)
    for h in range(2):
        piece = back[h * width : (h + 1) * width]
        for part in (first_ref, rest_ref):
            total = total + dot(piece, part[h * count : (h + 1) * count])
    out_ref[...] = total.astype(BF16)


def call(kernel, out_shapes, *args, flops=1 << 24, scratch=(), space=pltpu.VMEM, vmem=16):
    single = not isinstance(out_shapes, list)
    outs = [out_shapes] if single else out_shapes
    out_specs = [pl.BlockSpec(memory_space=pltpu.VMEM)] * len(outs)
    return pl.pallas_call(
        kernel,
        out_shape=out_shapes,
        in_specs=[pl.BlockSpec(memory_space=space)] * len(args),
        out_specs=out_specs[0] if single else out_specs,
        scratch_shapes=list(scratch),
        cost_estimate=pl.CostEstimate(flops=flops, bytes_accessed=1 << 20, transcendentals=0),
        compiler_params=pltpu.CompilerParams(vmem_limit_bytes=vmem << 20),
    )(*args)


def gathered(shard, axis):
    count = lax.axis_size(axis)
    me = lax.axis_index(axis)
    whole = jnp.zeros((count,) + shard.shape, shard.dtype)
    whole = lax.dynamic_update_slice_in_dim(whole, shard[None], me, 0)
    for hop in range(1, count):
        piece = lax.ppermute(shard, axis, [(i, (i + hop) % count) for i in range(count)])
        source = lax.rem(me + (count - hop), count)
        whole = lax.dynamic_update_slice_in_dim(whole, piece[None], source, 0)
    return whole


def body(tokens, norm_gain, gate_weight, up_weight, down_weight, expert_ids, route_weight):
    tok_rows, top = expert_ids.shape
    width = tokens.shape[1]
    full = norm_gain.shape[0]
    nz, cores, ny, nx = (lax.axis_size(axis) for axis in (Z, CORE, TY, TX))
    ep, tp = nz * cores, ny * nx
    units = gate_weight.shape[2]
    half = tok_rows * top // ep
    inner = half // nx
    count, wide = ep * half, 2 * width
    group = count // nx
    shape = jax.ShapeDtypeStruct

    sent, place, shard = call(
        functools.partial(prep_kernel, (nz, cores, nx)),
        [
            shape((count, wide), BF16),
            shape((top, tok_rows), I32),
            shape((3, units, full), BF16),
        ],
        expert_ids.T,
        tokens.T,
        gate_weight[0].T,
        up_weight[0].T,
        down_weight[0].T,
        scratch=(
            pltpu.VMEM((top, tok_rows), I32),
            pltpu.VMEM((width, tok_rows), BF16),
            pltpu.SemaphoreType.DMA((5,)),
        ),
        space=pltpu.HBM,
        vmem=62,
    )
    got = lax.all_to_all(
        sent.reshape(nz * nx, cores * inner, wide), (Z, TX), 0, 0, tiled=True
    )
    weights = gathered(shard, TX)

    spread = call(
        functools.partial(spread_kernel, (nz, nx, cores, inner)),
        shape((cores, ny, nx, nz * inner, wide), BF16),
        got.reshape(count, wide),
    )
    rows = lax.all_to_all(
        spread.reshape(cores * ny, nx * nz * inner, wide), (CORE, TY), 0, 0, tiled=True
    )
    hidden = call(
        up_kernel,
        shape((ny, 2 * group, nx * units), BF16),
        rows.reshape(cores, tp, nz * inner, wide),
        norm_gain.astype(F32).reshape(1, full),
        weights,
        flops=1 << 28,
        scratch=(pltpu.VMEM((2 * group, full), F32), pltpu.VMEM((2 * group, full), BF16)),
    )
    hidden = lax.all_to_all(hidden, TY, 0, 0, tiled=True)
    out = call(
        functools.partial(down_kernel, (nx, cores, nz, inner)),
        shape((count, wide), BF16),
        hidden,
        weights,
        flops=1 << 27,
    )

    back = lax.all_to_all(
        out.reshape(ep * nx, inner, wide), (Z, CORE, TX), 0, 0, tiled=True
    )
    first, rest = call(
        mix_kernel,
        [shape((2 * count, tok_rows), BF16)] * 2,
        place,
        route_weight.astype(F32).T,
    )
    combined = call(
        combine_kernel, shape((width, tok_rows), BF16), back.reshape(count, wide), first, rest
    )
    return combined.T


def solution(mesh):
    devices = mesh.devices.reshape(mesh.shape["ep"] // 2, 2, 4, 4)
    split = Mesh(devices, (Z, CORE, TY, TX))
    in_specs = (
        P(EP, TP),
        P(),
        P(EP, None, TP),
        P(EP, None, TP),
        P(EP, None, TP),
        P(EP, None),
        P(EP, None),
    )
    return jax.shard_map(body, mesh=split, in_specs=in_specs, out_specs=P(EP, TP), check_vma=False)
```

profile of v0, /device:TPU:1, one launch (start us, length us, event | category | flops | bytes accessed | tf_op | source)
XLA Modules:
  0.0 98.7 jit_solution(17696417913545833304)
XLA Ops:
  0.0 2.3 %shard_map.73 = (bf16[512,128]{1,0:T(8,128)(2,1)}, s32[4,128]{1,0:T(4,128)}, bf16[3,64,1024]{2,1,0:T(8,128)(2,1)}) custom-call(s32[4,128]{1,0:T(4,128)} %bitcast.38, bf16[64,128]{1,0:T(8,128)(2,1)} %bitcast.37, bf16[64,1024]{1,0:T(8,128)(2,1)} %bitcast.33, bf16[64,1024]{1,0:T(8,128)(2,1)} %bitcast.34, bf16[64,1024]{1,0:T(8,128)(2,1)} %bitcast.35), custom_call_target="tpu_custom_call" | custom-call | flops 16777216 | bytes 1048576 | tf_op jit(solution)/shard_map/pallas_call | solution.py:187
  2.3 0.0 copy-start.3
  2.3 4.1 %collective-permute-start = (bf16[3,64,1024]{2,1,0:T(8,128)(2,1)}, bf16[3,64,1024]{2,1,0:T(8,128)(2,1)S(1)}, u32[]{:S(2)}, u32[]{:S(2)}) collective-permute-start(bf16[3,64,1024]{2,1,0:T(8,128)(2,1)} %get-tuple-element.11), channel_id=1, source_target_pairs={{0,1},{1,2},{2,3},{3,0},{4,5},{5,6},{6,7},{7,4},{8,9},{9,10},{10,1... | collective-permute-start | bytes 1179656 | tf_op jit(solution)/shard_map/ppermute | solution.py:204
  6.4 18.0 %all-to-all-start = ((bf16[64,8,128]{2,1,0:T(8,128)(2,1)}), bf16[64,8,128]{2,1,0:T(8,128)(2,1)S(1)}, u32[]{:S(2)}, u32[]{:S(2)}) async-start(bf16[64,8,128]{2,1,0:T(8,128)(2,1)} %bitcast.36), calls=%async_computation | async-start | bytes 262144 | tf_op jit(solution)/shard_map/all_to_all | solution.py:243
  24.4 4.4 %collective-permute-start.1 = (bf16[3,64,1024]{2,1,0:T(8,128)(2,1)}, bf16[3,64,1024]{2,1,0:T(8,128)(2,1)S(1)}, u32[]{:S(2)}, u32[]{:S(2)}) collective-permute-start(bf16[3,64,1024]{2,1,0:T(8,128)(2,1)} %get-tuple-element.11), channel_id=1, source_target_pairs={{0,2},{1,3},{2,0},{3,1},{4,6},{5,7},{6,4},{7,5},{8,10},{9,11},{10,... | collective-permute-start | bytes 1179656 | tf_op jit(solution)/shard_map/ppermute | solution.py:204
  28.8 2.8 %collective-permute-start.2 = (bf16[3,64,1024]{2,1,0:T(8,128)(2,1)}, bf16[3,64,1024]{2,1,0:T(8,128)(2,1)S(1)}, u32[]{:S(2)}, u32[]{:S(2)}) collective-permute-start(bf16[3,64,1024]{2,1,0:T(8,128)(2,1)} %get-tuple-element.11), channel_id=1, source_target_pairs={{0,3},{1,0},{2,1},{3,2},{4,7},{5,4},{6,5},{7,6},{8,11},{9,8},{10,9... | collective-permute-start | bytes 1179656 | tf_op jit(solution)/shard_map/ppermute | solution.py:204
  31.7 0.2 broadcast_in_dim.15
  31.8 0.0 copy-done.3
  31.9 0.0 collective-permute-done
  32.0 7.8 %all-to-all-done = bf16[64,8,128]{2,1,0:T(8,128)(2,1)S(1)} async-done(((bf16[64,8,128]{2,1,0:T(8,128)(2,1)}), bf16[64,8,128]{2,1,0:T(8,128)(2,1)S(1)}, u32[]{:S(2)}, u32[]{:S(2)}) %all-to-all-start) | async-done | bytes 131104 | tf_op jit(solution)/shard_map/all_to_all | solution.py:243
  39.8 0.0 copy-start
  39.8 1.1 %shard_map.74 = bf16[2,4,4,64,128]{4,3,2,1,0:T(8,128)(2,1)} custom-call(bf16[512,128]{1,0:T(8,128)(2,1)S(1)} %bitcast.29), custom_call_target="tpu_custom_call" | custom-call | flops 16777216 | bytes 1048576 | tf_op jit(solution)/shard_map/pallas_call | solution.py:187
  40.9 7.7 %all-to-all-start.1 = ((bf16[8,256,128]{2,1,0:T(8,128)(2,1)}), bf16[8,256,128]{2,1,0:T(8,128)(2,1)S(1)}, u32[]{:S(2)}, u32[]{:S(2)}) async-start(bf16[8,256,128]{2,1,0:T(8,128)(2,1)} %bitcast.10), calls=%async_computation.1 | async-start | bytes 1048576 | tf_op jit(solution)/shard_map/all_to_all | solution.py:253
  48.6 0.0 collective-permute-done.1
  48.6 0.0 collective-permute-done.2
  48.7 9.2 %all-to-all-done.1 = bf16[8,256,128]{2,1,0:T(8,128)(2,1)S(1)} async-done(((bf16[8,256,128]{2,1,0:T(8,128)(2,1)}), bf16[8,256,128]{2,1,0:T(8,128)(2,1)S(1)}, u32[]{:S(2)}, u32[]{:S(2)}) %all-to-all-start.1) | async-done | bytes 524320 | tf_op jit(solution)/shard_map/all_to_all | solution.py:253
  57.9 0.0 copy-done
  57.9 0.9 shard_map.75
  58.8 0.0 copy-start.1
  58.8 0.0 copy-start.2
  58.8 10.9 %all_to_all.20.hidden_ref = bf16[4,256,256]{2,1,0:T(8,128)(2,1)S(1)} all-to-all(bf16[4,256,256]{2,1,0:T(8,128)(2,1)S(1)} %shard_map.75), channel_id=1, replica_groups=mesh['z'=16,'core'=2,'ty'=4,'tx'=4] {'ty'}, dimensions={0} | all-to-all | bytes 1048576 | tf_op jit(solution)/shard_map/all_to_all | solution.py:265
  69.7 1.6 %shard_map.76 = bf16[512,128]{1,0:T(8,128)(2,1)} custom-call(bf16[4,256,256]{2,1,0:T(8,128)(2,1)S(1)} %all_to_all.20.hidden_ref, bf16[4,3,64,1024]{3,2,1,0:T(8,128)(2,1)S(1)} %bitcast_dynamic-update-slice_fusion.weights_ref), custom_call_target="tpu_custom_call" | custom-call | flops 134217728 | bytes 1048576 | tf_op jit(solution)/shard_map/pallas_call | solution.py:187
  71.3 8.3 %all-to-all-start.3 = ((bf16[128,4,128]{2,1,0:T(4,128)(2,1)}), bf16[128,4,128]{2,1,0:T(4,128)(2,1)S(1)}, u32[]{:S(2)}, u32[]{:S(2)}) async-start(bf16[128,4,128]{2,1,0:T(4,128)(2,1)} %bitcast.17), calls=%async_computation.3 | async-start | bytes 262144 | tf_op jit(solution)/shard_map/all_to_all | solution.py:274
  79.7 0.0 copy-done.1
  79.7 0.0 copy-done.2
  79.7 0.3 shard_map.77
  79.9 17.8 %all-to-all-done.3 = bf16[128,4,128]{2,1,0:T(4,128)(2,1)S(1)} async-done(((bf16[128,4,128]{2,1,0:T(4,128)(2,1)}), bf16[128,4,128]{2,1,0:T(4,128)(2,1)S(1)}, u32[]{:S(2)}, u32[]{:S(2)}) %all-to-all-start.3) | async-done | bytes 131104 | tf_op jit(solution)/shard_map/all_to_all | solution.py:274
  97.8 0.9 shard_map.78
  (4 shorter events, 0.1 us)
Async XLA Ops:
  2.3 29.5 %copy-start.3 = (bf16[3,64,1024]{2,1,0:T(8,128)(2,1)S(1)}, bf16[3,64,1024]{2,1,0:T(8,128)(2,1)}, u32[]{:S(2)}) copy-start(bf16[3,64,1024]{2,1,0:T(8,128)(2,1)} %get-tuple-element.11) | copy-start | bytes 1179652
  2.3 29.6 %collective-permute-start = (bf16[3,64,1024]{2,1,0:T(8,128)(2,1)}, bf16[3,64,1024]{2,1,0:T(8,128)(2,1)S(1)}, u32[]{:S(2)}, u32[]{:S(2)}) collective-permute-start(bf16[3,64,1024]{2,1,0:T(8,128)(2,1)} %get-tuple-element.11), channel_id=1, source_target_pairs={{0,1},{1,2},{2,3},{3,0},{4,5},{5,6},{6,7},{7,4},{8,9},{9,10},{10,1... | collective-permute-start | bytes 1179656 | tf_op jit(solution)/shard_map/ppermute | solution.py:204
  6.4 33.4 %all-to-all-start = ((bf16[64,8,128]{2,1,0:T(8,128)(2,1)}), bf16[64,8,128]{2,1,0:T(8,128)(2,1)S(1)}, u32[]{:S(2)}, u32[]{:S(2)}) async-start(bf16[64,8,128]{2,1,0:T(8,128)(2,1)} %bitcast.36), calls=%async_computation | async-start | bytes 262144 | tf_op jit(solution)/shard_map/all_to_all | solution.py:243
  24.4 24.2 %collective-permute-start.1 = (bf16[3,64,1024]{2,1,0:T(8,128)(2,1)}, bf16[3,64,1024]{2,1,0:T(8,128)(2,1)S(1)}, u32[]{:S(2)}, u32[]{:S(2)}) collective-permute-start(bf16[3,64,1024]{2,1,0:T(8,128)(2,1)} %get-tuple-element.11), channel_id=1, source_target_pairs={{0,2},{1,3},{2,0},{3,1},{4,6},{5,7},{6,4},{7,5},{8,10},{9,11},{10,... | collective-permute-start | bytes 1179656 | tf_op jit(solution)/shard_map/ppermute | solution.py:204
  28.8 19.8 %collective-permute-start.2 = (bf16[3,64,1024]{2,1,0:T(8,128)(2,1)}, bf16[3,64,1024]{2,1,0:T(8,128)(2,1)S(1)}, u32[]{:S(2)}, u32[]{:S(2)}) collective-permute-start(bf16[3,64,1024]{2,1,0:T(8,128)(2,1)} %get-tuple-element.11), channel_id=1, source_target_pairs={{0,3},{1,0},{2,1},{3,2},{4,7},{5,4},{6,5},{7,6},{8,11},{9,8},{10,9... | collective-permute-start | bytes 1179656 | tf_op jit(solution)/shard_map/ppermute | solution.py:204
  39.8 18.2 %copy-start = (f32[1024]{0:T(1024)S(1)}, f32[1024]{0:T(1024)}, u32[]{:S(2)}) copy-start(f32[1024]{0:T(1024)} %param.8) | copy-start | bytes 12292
  40.9 17.0 %all-to-all-start.1 = ((bf16[8,256,128]{2,1,0:T(8,128)(2,1)}), bf16[8,256,128]{2,1,0:T(8,128)(2,1)S(1)}, u32[]{:S(2)}, u32[]{:S(2)}) async-start(bf16[8,256,128]{2,1,0:T(8,128)(2,1)} %bitcast.10), calls=%async_computation.1 | async-start | bytes 1048576 | tf_op jit(solution)/shard_map/all_to_all | solution.py:253
  58.8 20.9 %copy-start.1 = (f32[128,4]{0,1:T(4,128)S(1)}, f32[128,4]{0,1:T(4,128)}, u32[]{:S(2)}) copy-start(f32[128,4]{0,1:T(4,128)} %param.13) | copy-start | bytes 6148
  58.8 20.9 %copy-start.2 = (s32[4,128]{1,0:T(4,128)S(1)}, s32[4,128]{1,0:T(4,128)}, u32[]{:S(2)}) copy-start(s32[4,128]{1,0:T(4,128)} %get-tuple-element.12.place_ref) | copy-start | bytes 6148
  71.3 26.5 %all-to-all-start.3 = ((bf16[128,4,128]{2,1,0:T(4,128)(2,1)}), bf16[128,4,128]{2,1,0:T(4,128)(2,1)S(1)}, u32[]{:S(2)}, u32[]{:S(2)}) async-start(bf16[128,4,128]{2,1,0:T(4,128)(2,1)} %bitcast.17), calls=%async_computation.3 | async-start | bytes 262144 | tf_op jit(solution)/shard_map/all_to_all | solution.py:274
where the time goes:
time: 99.1 us; the launch traced here: 98.7 us
  starting transfers between devices  45.3 us (46%)
  waiting for transfers between devices  34.9 us (35%)
  blocking collectives  10.9 us (11%)
  Pallas kernels  7.01 us (7%)
    all_to_all x1, starting transfers between devices, body(): lax.all_to_all(sent.reshape(nz * nx, cores * inner, wide), (Z, TX), 0, 0,...  18 us
    all_to_all x1, waiting for transfers between devices, body(): lax.all_to_all(out.reshape(ep * nx, inner, wide), (Z, CORE, TX), 0, 0, ti...  17.8 us
    ppermute x3, starting transfers between devices, gathered(): lax.ppermute(shard, axis, [(i, (i + hop) % count) for i in range(count)])  11.3 us
    all_to_all x1, blocking collectives, body(): hidden = lax.all_to_all(hidden, TY, 0, 0, tiled=True)  10.9 us
    all_to_all x1, waiting for transfers between devices, body(): lax.all_to_all(spread.reshape(cores * ny, nx * nz * inner, wide), (CORE,...  9.24 us
    all_to_all x1, starting transfers between devices, body(): lax.all_to_all(out.reshape(ep * nx, inner, wide), (Z, CORE, TX), 0, 0, ti...  8.35 us
    all_to_all x1, waiting for transfers between devices, body(): lax.all_to_all(sent.reshape(nz * nx, cores * inner, wide), (Z, TX), 0, 0,...  7.8 us
    all_to_all x1, starting transfers between devices, body(): lax.all_to_all(spread.reshape(cores * ny, nx * nz * inner, wide), (CORE,...  7.7 us
  transfers between devices with their start and end apart: 6, of which 3 were waited for; matrix products, arithmetic and copies ran while one was open for 0% of the time, Pallas kernels for 1%

commit v1 on v0

--- a/solution.py
+++ b/solution.py
@@ -34,17 +34,13 @@
     return jnp.where(mask, 1.0, 0.0).astype(BF16)
 
 
-def moved(rows, sizes, order):
-    count = rows.shape[0]
-    left, source = iota((count, 1), 0), jnp.zeros((count, 1), I32)
-    for axis in reversed(order):
-        stride = 1
-        for size in sizes[axis + 1 :]:
-            stride *= size
-        source = source + (left & (sizes[axis] - 1)) * stride
-        left = left >> (sizes[axis].bit_length() - 1)
-    select = ones_where(iota((count, count), 1) == source)
-    return dot(select, rows).astype(BF16)
+def quads(first, second):
+    half = first.shape[1] // 2
+    top = iota(first.shape, 1) < half
+    return (
+        jnp.where(top, first, pltpu.roll(second, half, 1)),
+        jnp.where(top, pltpu.roll(first, half, 1), second),
+    )
 
 
 def halves(first, second):
@@ -115,12 +111,17 @@
     rest_ref[...] = (mix - first.astype(F32)).astype(BF16)
 
 
-def spread_kernel(sizes, got_ref, out_ref):
-    cores, copies, _, _, _ = out_ref.shape
-    rows = moved(got_ref[...], sizes, (2, 1, 0, 3)).reshape((cores,) + out_ref.shape[2:])
+def spread_kernel(got_ref, out_ref, turned):
+    cores, copies, nx, rows, wide = out_ref.shape
+    got = got_ref[...].astype(F32).reshape(-1, 2, nx, 8, wide)
+    for x in range(nx):
+        for core, part in enumerate(quads(got[:, 0, x], got[:, 1, x])):
+            turned[core, x] = part.reshape(rows, wide)
     for core in range(cores):
-        for c in range(copies):
-            out_ref[core, c] = rows[core]
+        for x in range(nx):
+            part = turned[core, x].astype(BF16)
+            for c in range(copies):
+                out_ref[core, c, x] = part
 
 
 def up_kernel(rows_ref, gain_ref, weights_ref, out_ref, whole, normed):
@@ -152,7 +153,7 @@
         out_ref[c] = hidden
 
 
-def down_kernel(sizes, hidden_ref, weights_ref, out_ref):
+def down_kernel(cores, hidden_ref, weights_ref, out_ref, turned):
     ny, rows, units = hidden_ref.shape
     nx, _, width, full = weights_ref.shape
     w_down = weights_ref[:, 2].reshape(nx * width, full)
@@ -164,8 +165,13 @@
     for j in range(nx // 2):
         lanes = slice(2 * j * width, 2 * (j + 1) * width)
         pieces += halves(total[:group, lanes], total[group:, lanes])
-    stacked = jnp.concatenate(pieces, 0).astype(BF16)
-    out_ref[...] = moved(stacked, sizes, (2, 1, 0, 3))
+    for j in range(nx // 2):
+        first, second = (p.reshape(-1, 8, 2 * width) for p in pieces[2 * j : 2 * j + 2])
+        for odd, part in enumerate(quads(first, second)):
+            part = part.reshape(cores, -1, 8, 2 * width)
+            for core in range(cores):
+                turned[:, odd, core, j] = part[core]
+    out_ref[...] = turned[...].reshape(out_ref.shape).astype(BF16)
 
 
 def combine_kernel(back_ref, first_ref, rest_ref, out_ref):
@@ -246,9 +252,10 @@
     weights = gathered(shard, TX)
 
     spread = call(
-        functools.partial(spread_kernel, (nz, nx, cores, inner)),
+        spread_kernel,
         shape((cores, ny, nx, nz * inner, wide), BF16),
         got.reshape(count, wide),
+        scratch=(pltpu.VMEM((cores, nx, nz * inner, wide), F32),),
     )
     rows = lax.all_to_all(
         spread.reshape(cores * ny, nx * nz * inner, wide), (CORE, TY), 0, 0, tiled=True
@@ -264,11 +271,12 @@
     )
     hidden = lax.all_to_all(hidden, TY, 0, 0, tiled=True)
     out = call(
-        functools.partial(down_kernel, (nx, cores, nz, inner)),
+        functools.partial(down_kernel, cores),
         shape((count, wide), BF16),
         hidden,
         weights,
         flops=1 << 27,
+        scratch=(pltpu.VMEM((nz // 2, 2, cores, nx // 2, 2 * inner, wide), F32),),
     )
 
     back = lax.all_to_all(

time: 99.1 us -> 98.6 us (level)
  no operation moved by 1% of the time
where the time goes in v1:
time: 98.6 us; the launch traced here: 98.2 us
  starting transfers between devices  45.6 us (46%)
  waiting for transfers between devices  34.9 us (35%)
  blocking collectives  10.9 us (11%)
  Pallas kernels  6.21 us (6%)
    all_to_all x1, starting transfers between devices, body(): lax.all_to_all(sent.reshape(nz * nx, cores * inner, wide), (Z, TX), 0, 0,...  18 us
    all_to_all x1, waiting for transfers between devices, body(): lax.all_to_all(out.reshape(ep * nx, inner, wide), (Z, CORE, TX), 0, 0, ti...  17.8 us
    ppermute x3, starting transfers between devices, gathered(): lax.ppermute(shard, axis, [(i, (i + hop) % count) for i in range(count)])  11.3 us
    all_to_all x1, blocking collectives, body(): hidden = lax.all_to_all(hidden, TY, 0, 0, tiled=True)  10.9 us
    all_to_all x1, waiting for transfers between devices, body(): lax.all_to_all(spread.reshape(cores * ny, nx * nz * inner, wide), (CORE,...  9.24 us
    all_to_all x1, starting transfers between devices, body(): lax.all_to_all(out.reshape(ep * nx, inner, wide), (Z, CORE, TX), 0, 0, ti...  8.62 us
    all_to_all x1, waiting for transfers between devices, body(): lax.all_to_all(sent.reshape(nz * nx, cores * inner, wide), (Z, TX), 0, 0,...  7.8 us
    all_to_all x1, starting transfers between devices, body(): lax.all_to_all(spread.reshape(cores * ny, nx * nz * inner, wide), (CORE,...  7.7 us
  transfers between devices with their start and end apart: 6, of which 3 were waited for; matrix products, arithmetic and copies ran while one was open for 0% of the time, Pallas kernels for 1%

profile of v1, /device:TPU:1, one launch (start us, length us, event | category | flops | bytes accessed | tf_op | source)
XLA Modules:
  0.0 98.2 jit_solution(3787305617467288944)
XLA Ops:
  0.0 2.3 %shard_map.73 = (bf16[512,128]{1,0:T(8,128)(2,1)}, s32[4,128]{1,0:T(4,128)}, bf16[3,64,1024]{2,1,0:T(8,128)(2,1)}) custom-call(s32[4,128]{1,0:T(4,128)} %bitcast.38, bf16[64,128]{1,0:T(8,128)(2,1)} %bitcast.37, bf16[64,1024]{1,0:T(8,128)(2,1)} %bitcast.33, bf16[64,1024]{1,0:T(8,128)(2,1)} %bitcast.34, bf16[64,1024]{1,0:T(8,128)(2,1)} %bitcast.35), custom_call_target="tpu_custom_call" | custom-call | flops 16777216 | bytes 1048576 | tf_op jit(solution)/shard_map/pallas_call | solution.py:193
  2.3 0.0 copy-start.3
  2.3 4.1 %collective-permute-start = (bf16[3,64,1024]{2,1,0:T(8,128)(2,1)}, bf16[3,64,1024]{2,1,0:T(8,128)(2,1)S(1)}, u32[]{:S(2)}, u32[]{:S(2)}) collective-permute-start(bf16[3,64,1024]{2,1,0:T(8,128)(2,1)} %get-tuple-element.11), channel_id=1, source_target_pairs={{0,1},{1,2},{2,3},{3,0},{4,5},{5,6},{6,7},{7,4},{8,9},{9,10},{10,1... | collective-permute-start | bytes 1179656 | tf_op jit(solution)/shard_map/ppermute | solution.py:210
  6.4 18.0 %all-to-all-start = ((bf16[64,8,128]{2,1,0:T(8,128)(2,1)}), bf16[64,8,128]{2,1,0:T(8,128)(2,1)S(1)}, u32[]{:S(2)}, u32[]{:S(2)}) async-start(bf16[64,8,128]{2,1,0:T(8,128)(2,1)} %bitcast.36), calls=%async_computation | async-start | bytes 262144 | tf_op jit(solution)/shard_map/all_to_all | solution.py:249
  24.4 4.4 %collective-permute-start.1 = (bf16[3,64,1024]{2,1,0:T(8,128)(2,1)}, bf16[3,64,1024]{2,1,0:T(8,128)(2,1)S(1)}, u32[]{:S(2)}, u32[]{:S(2)}) collective-permute-start(bf16[3,64,1024]{2,1,0:T(8,128)(2,1)} %get-tuple-element.11), channel_id=1, source_target_pairs={{0,2},{1,3},{2,0},{3,1},{4,6},{5,7},{6,4},{7,5},{8,10},{9,11},{10,... | collective-permute-start | bytes 1179656 | tf_op jit(solution)/shard_map/ppermute | solution.py:210
  28.8 2.8 %collective-permute-start.2 = (bf16[3,64,1024]{2,1,0:T(8,128)(2,1)}, bf16[3,64,1024]{2,1,0:T(8,128)(2,1)S(1)}, u32[]{:S(2)}, u32[]{:S(2)}) collective-permute-start(bf16[3,64,1024]{2,1,0:T(8,128)(2,1)} %get-tuple-element.11), channel_id=1, source_target_pairs={{0,3},{1,0},{2,1},{3,2},{4,7},{5,4},{6,5},{7,6},{8,11},{9,8},{10,9... | collective-permute-start | bytes 1179656 | tf_op jit(solution)/shard_map/ppermute | solution.py:210
  31.7 0.2 broadcast_in_dim.15
  31.8 0.0 copy-done.3
  31.9 0.0 collective-permute-done
  32.0 7.8 %all-to-all-done = bf16[64,8,128]{2,1,0:T(8,128)(2,1)S(1)} async-done(((bf16[64,8,128]{2,1,0:T(8,128)(2,1)}), bf16[64,8,128]{2,1,0:T(8,128)(2,1)S(1)}, u32[]{:S(2)}, u32[]{:S(2)}) %all-to-all-start) | async-done | bytes 131104 | tf_op jit(solution)/shard_map/all_to_all | solution.py:249
  39.8 0.0 copy-start
  39.8 0.8 shard_map.74
  40.6 7.7 %all-to-all-start.1 = ((bf16[8,256,128]{2,1,0:T(8,128)(2,1)}), bf16[8,256,128]{2,1,0:T(8,128)(2,1)S(1)}, u32[]{:S(2)}, u32[]{:S(2)}) async-start(bf16[8,256,128]{2,1,0:T(8,128)(2,1)} %bitcast.10), calls=%async_computation.1 | async-start | bytes 1048576 | tf_op jit(solution)/shard_map/all_to_all | solution.py:260
  48.3 0.0 collective-permute-done.1
  48.3 0.0 collective-permute-done.2
  48.4 9.2 %all-to-all-done.1 = bf16[8,256,128]{2,1,0:T(8,128)(2,1)S(1)} async-done(((bf16[8,256,128]{2,1,0:T(8,128)(2,1)}), bf16[8,256,128]{2,1,0:T(8,128)(2,1)S(1)}, u32[]{:S(2)}, u32[]{:S(2)}) %all-to-all-start.1) | async-done | bytes 524320 | tf_op jit(solution)/shard_map/all_to_all | solution.py:260
  57.6 0.0 copy-done
  57.6 0.9 shard_map.75
  58.5 0.0 copy-start.1
  58.5 0.0 copy-start.2
  58.5 10.9 %all_to_all.20.hidden_ref = bf16[4,256,256]{2,1,0:T(8,128)(2,1)S(1)} all-to-all(bf16[4,256,256]{2,1,0:T(8,128)(2,1)S(1)} %shard_map.75), channel_id=1, replica_groups=mesh['z'=16,'core'=2,'ty'=4,'tx'=4] {'ty'}, dimensions={0} | all-to-all | bytes 1048576 | tf_op jit(solution)/shard_map/all_to_all | solution.py:272
  69.4 1.1 %shard_map.76 = bf16[512,128]{1,0:T(8,128)(2,1)} custom-call(bf16[4,256,256]{2,1,0:T(8,128)(2,1)S(1)} %all_to_all.20.hidden_ref, bf16[4,3,64,1024]{3,2,1,0:T(8,128)(2,1)S(1)} %bitcast_dynamic-update-slice_fusion.weights_ref), custom_call_target="tpu_custom_call" | custom-call | flops 134217728 | bytes 1048576 | tf_op jit(solution)/shard_map/pallas_call | solution.py:193
  70.5 8.6 %all-to-all-start.3 = ((bf16[128,4,128]{2,1,0:T(4,128)(2,1)}), bf16[128,4,128]{2,1,0:T(4,128)(2,1)S(1)}, u32[]{:S(2)}, u32[]{:S(2)}) async-start(bf16[128,4,128]{2,1,0:T(4,128)(2,1)} %bitcast.17), calls=%async_computation.3 | async-start | bytes 262144 | tf_op jit(solution)/shard_map/all_to_all | solution.py:282
  79.1 0.0 copy-done.1
  79.1 0.0 copy-done.2
  79.2 0.3 shard_map.77
  79.4 17.8 %all-to-all-done.3 = bf16[128,4,128]{2,1,0:T(4,128)(2,1)S(1)} async-done(((bf16[128,4,128]{2,1,0:T(4,128)(2,1)}), bf16[128,4,128]{2,1,0:T(4,128)(2,1)S(1)}, u32[]{:S(2)}, u32[]{:S(2)}) %all-to-all-start.3) | async-done | bytes 131104 | tf_op jit(solution)/shard_map/all_to_all | solution.py:282
  97.3 0.9 shard_map.78
  (4 shorter events, 0.1 us)
Async XLA Ops:
  2.3 29.5 %copy-start.3 = (bf16[3,64,1024]{2,1,0:T(8,128)(2,1)S(1)}, bf16[3,64,1024]{2,1,0:T(8,128)(2,1)}, u32[]{:S(2)}) copy-start(bf16[3,64,1024]{2,1,0:T(8,128)(2,1)} %get-tuple-element.11) | copy-start | bytes 1179652
  2.3 29.6 %collective-permute-start = (bf16[3,64,1024]{2,1,0:T(8,128)(2,1)}, bf16[3,64,1024]{2,1,0:T(8,128)(2,1)S(1)}, u32[]{:S(2)}, u32[]{:S(2)}) collective-permute-start(bf16[3,64,1024]{2,1,0:T(8,128)(2,1)} %get-tuple-element.11), channel_id=1, source_target_pairs={{0,1},{1,2},{2,3},{3,0},{4,5},{5,6},{6,7},{7,4},{8,9},{9,10},{10,1... | collective-permute-start | bytes 1179656 | tf_op jit(solution)/shard_map/ppermute | solution.py:210
  6.4 33.4 %all-to-all-start = ((bf16[64,8,128]{2,1,0:T(8,128)(2,1)}), bf16[64,8,128]{2,1,0:T(8,128)(2,1)S(1)}, u32[]{:S(2)}, u32[]{:S(2)}) async-start(bf16[64,8,128]{2,1,0:T(8,128)(2,1)} %bitcast.36), calls=%async_computation | async-start | bytes 262144 | tf_op jit(solution)/shard_map/all_to_all | solution.py:249
  24.4 23.9 %collective-permute-start.1 = (bf16[3,64,1024]{2,1,0:T(8,128)(2,1)}, bf16[3,64,1024]{2,1,0:T(8,128)(2,1)S(1)}, u32[]{:S(2)}, u32[]{:S(2)}) collective-permute-start(bf16[3,64,1024]{2,1,0:T(8,128)(2,1)} %get-tuple-element.11), channel_id=1, source_target_pairs={{0,2},{1,3},{2,0},{3,1},{4,6},{5,7},{6,4},{7,5},{8,10},{9,11},{10,... | collective-permute-start | bytes 1179656 | tf_op jit(solution)/shard_map/ppermute | solution.py:210
  28.8 19.5 %collective-permute-start.2 = (bf16[3,64,1024]{2,1,0:T(8,128)(2,1)}, bf16[3,64,1024]{2,1,0:T(8,128)(2,1)S(1)}, u32[]{:S(2)}, u32[]{:S(2)}) collective-permute-start(bf16[3,64,1024]{2,1,0:T(8,128)(2,1)} %get-tuple-element.11), channel_id=1, source_target_pairs={{0,3},{1,0},{2,1},{3,2},{4,7},{5,4},{6,5},{7,6},{8,11},{9,8},{10,9... | collective-permute-start | bytes 1179656 | tf_op jit(solution)/shard_map/ppermute | solution.py:210
  39.8 17.9 %copy-start = (f32[1024]{0:T(1024)S(1)}, f32[1024]{0:T(1024)}, u32[]{:S(2)}) copy-start(f32[1024]{0:T(1024)} %param.8) | copy-start | bytes 12292
  40.6 17.0 %all-to-all-start.1 = ((bf16[8,256,128]{2,1,0:T(8,128)(2,1)}), bf16[8,256,128]{2,1,0:T(8,128)(2,1)S(1)}, u32[]{:S(2)}, u32[]{:S(2)}) async-start(bf16[8,256,128]{2,1,0:T(8,128)(2,1)} %bitcast.10), calls=%async_computation.1 | async-start | bytes 1048576 | tf_op jit(solution)/shard_map/all_to_all | solution.py:260
  58.5 20.6 %copy-start.1 = (f32[128,4]{0,1:T(4,128)S(1)}, f32[128,4]{0,1:T(4,128)}, u32[]{:S(2)}) copy-start(f32[128,4]{0,1:T(4,128)} %param.13) | copy-start | bytes 6148
  58.5 20.6 %copy-start.2 = (s32[4,128]{1,0:T(4,128)S(1)}, s32[4,128]{1,0:T(4,128)}, u32[]{:S(2)}) copy-start(s32[4,128]{1,0:T(4,128)} %get-tuple-element.12.place_ref) | copy-start | bytes 6148
  70.5 26.8 %all-to-all-start.3 = ((bf16[128,4,128]{2,1,0:T(4,128)(2,1)}), bf16[128,4,128]{2,1,0:T(4,128)(2,1)S(1)}, u32[]{:S(2)}, u32[]{:S(2)}) async-start(bf16[128,4,128]{2,1,0:T(4,128)(2,1)} %bitcast.17), calls=%async_computation.3 | async-start | bytes 262144 | tf_op jit(solution)/shard_map/all_to_all | solution.py:282

commit v2 on v1

--- a/solution.py
+++ b/solution.py
@@ -155,8 +155,8 @@
 
 def down_kernel(cores, hidden_ref, weights_ref, out_ref, turned):
     ny, rows, units = hidden_ref.shape
-    nx, _, width, full = weights_ref.shape
-    w_down = weights_ref[:, 2].reshape(nx * width, full)
+    nx, width, full = weights_ref.shape
+    w_down = weights_ref[...].reshape(nx * width, full)
     total = dot_nt(hidden_ref[0], w_down[:, :units])
     for y in range(1, ny):
         total = total + dot_nt(hidden_ref[y], w_down[:, y * units : (y + 1) * units])
@@ -201,16 +201,29 @@
     )(*args)
 
 
-def gathered(shard, axis):
-    count = lax.axis_size(axis)
-    me = lax.axis_index(axis)
-    whole = jnp.zeros((count,) + shard.shape, shard.dtype)
-    whole = lax.dynamic_update_slice_in_dim(whole, shard[None], me, 0)
-    for hop in range(1, count):
-        piece = lax.ppermute(shard, axis, [(i, (i + hop) % count) for i in range(count)])
-        source = lax.rem(me + (count - hop), count)
-        whole = lax.dynamic_update_slice_in_dim(whole, piece[None], source, 0)
-    return whole
+def set_at(whole, piece, index):
+    return lax.dynamic_update_slice_in_dim(whole, piece[None], index, 0)
+
+
+def gathered(shard):
+    count = lax.axis_size(TX)
+    me = lax.axis_index(TX)
+    near, after = ([(i, (i + hop) % count) for i in range(count)] for hop in (1, count - 1))
+    left = lax.ppermute(shard, TX, near)
+    right = lax.ppermute(shard, TX, after)
+    far_up = lax.ppermute(left[:2], TX, near)
+    far_down = lax.ppermute(right[2], TX, after)
+    up = jnp.zeros((count, 2) + shard.shape[1:], shard.dtype)
+    down = jnp.zeros((count,) + shard.shape[1:], shard.dtype)
+    up, down = set_at(up, shard[:2], me), set_at(down, shard[2], me)
+    before, behind, across = (lax.rem(me + hop, count) for hop in (count - 1, 1, count - 2))
+    for piece, source in ((left, before), (right, behind)):
+        up = set_at(up, piece[:2], source)
+    up = set_at(up, far_up, across)
+    for piece, source in ((left, before), (right, behind)):
+        down = set_at(down, piece[2], source)
+    down = set_at(down, far_down, across)
+    return up, down
 
 
 def body(tokens, norm_gain, gate_weight, up_weight, down_weight, expert_ids, route_weight):
@@ -249,7 +262,7 @@
     got = lax.all_to_all(
         sent.reshape(nz * nx, cores * inner, wide), (Z, TX), 0, 0, tiled=True
     )
-    weights = gathered(shard, TX)
+    w_up, w_down = gathered(shard)
 
     spread = call(
         spread_kernel,
@@ -265,7 +278,7 @@
         shape((ny, 2 * group, nx * units), BF16),
         rows.reshape(cores, tp, nz * inner, wide),
         norm_gain.astype(F32).reshape(1, full),
-        weights,
+        w_up,
         flops=1 << 28,
         scratch=(pltpu.VMEM((2 * group, full), F32), pltpu.VMEM((2 * group, full), BF16)),
     )
@@ -274,7 +287,7 @@
         functools.partial(down_kernel, cores),
         shape((count, wide), BF16),
         hidden,
-        weights,
+        w_down,
         flops=1 << 27,
         scratch=(pltpu.VMEM((nz // 2, 2, cores, nx // 2, 2 * inner, wide), F32),),
     )

time: 98.6 us -> 102 us (1.034)
  blocking collectives: 10.9 us -> 0 us
  waiting for transfers between devices: 34.9 us -> 44.3 us
  starting transfers between devices: 45.6 us -> 47.6 us
  local copies, waits for them, and re-layouts: 0.35 us -> 1.88 us
    all_to_all x1 -> x0, blocking collectives: 10.9 us -> none  [body(): hidden = lax.all_to_all(hidden, TY, 0, 0, tiled=True)]
    ppermute x3 -> x4, waiting for transfers between devices: 0.01 us -> 4.04 us  [the longest x1 4.03 us: gathered(): far_down = lax.ppermute(right[2], TX, after)]
    all_to_all x0 -> x1, starting transfers between devices: none -> 3.47 us  [body(): hidden = lax.all_to_all(hidden, TY, 0, 0, tiled=True)]
    all_to_all x1, waiting for transfers between devices: 7.8 us -> 11 us  [body(): lax.all_to_all(sent.reshape(nz * nx, cores * inner, wide), (Z, TX), 0, 0,...]
    all_to_all x0 -> x1, waiting for transfers between devices: none -> 2.54 us  [body(): hidden = lax.all_to_all(hidden, TY, 0, 0, tiled=True)]
    all_to_all x1, starting transfers between devices: 8.62 us -> 6.47 us  [body(): lax.all_to_all(out.reshape(ep * nx, inner, wide), (Z, CORE, TX), 0, 0, ti...]
    unnamed x8, local copies, waits for them, and re-layouts: 0.02 us -> 1.54 us
    ppermute x3 -> x4, starting transfers between devices: 11.3 us -> 12.7 us  [the longest x1 3.94 us: gathered(): left = lax.ppermute(shard, TX, near)]
  transfers between devices with their start and end apart: 6 -> 8, of which waited for: 3 -> 5; matrix products, arithmetic and copies ran while one was open for 0% -> 0% of each run, Pallas kernels for 1% -> 1%
where the time goes in v2:
time: 102 us; the launch traced here: 101 us
  starting transfers between devices  47.6 us (47%)
  waiting for transfers between devices  44.3 us (43%)
  Pallas kernels  7.04 us (7%)
  local copies, waits for them, and re-layouts  1.88 us (2%)
    all_to_all x1, waiting for transfers between devices, body(): lax.all_to_all(out.reshape(ep * nx, inner, wide), (Z, CORE, TX), 0, 0, ti...  17.4 us
    all_to_all x1, starting transfers between devices, body(): lax.all_to_all(sent.reshape(nz * nx, cores * inner, wide), (Z, TX), 0, 0,...  17.3 us
    all_to_all x1, waiting for transfers between devices, body(): lax.all_to_all(sent.reshape(nz * nx, cores * inner, wide), (Z, TX), 0, 0,...  11 us
    all_to_all x1, waiting for transfers between devices, body(): lax.all_to_all(spread.reshape(cores * ny, nx * nz * inner, wide), (CORE,...  9.27 us
    all_to_all x1, starting transfers between devices, body(): lax.all_to_all(spread.reshape(cores * ny, nx * nz * inner, wide), (CORE,...  7.78 us
    pallas_call x6, Pallas kernels, call(): pl.pallas_call(kernel, out_shape=out_shapes, in_specs=[pl.BlockSpec(memor...  7.04 us
    all_to_all x1, starting transfers between devices, body(): lax.all_to_all(out.reshape(ep * nx, inner, wide), (Z, CORE, TX), 0, 0, ti...  6.47 us
    ppermute x1, waiting for transfers between devices, gathered(): far_down = lax.ppermute(right[2], TX, after)  4.03 us
  transfers between devices with their start and end apart: 8, of which 5 were waited for; matrix products, arithmetic and copies ran while one was open for 0% of the time, Pallas kernels for 1%

profile of v2, /device:TPU:1, one launch (start us, length us, event | category | flops | bytes accessed | tf_op | source)
XLA Modules:
  0.0 101.1 jit_solution(12319072858892334767)
XLA Ops:
  0.0 2.3 %shard_map.73 = (bf16[512,128]{1,0:T(8,128)(2,1)}, s32[4,128]{1,0:T(4,128)}, bf16[3,64,1024]{2,1,0:T(8,128)(2,1)}) custom-call(s32[4,128]{1,0:T(4,128)} %bitcast.44, bf16[64,128]{1,0:T(8,128)(2,1)} %bitcast.43, bf16[64,1024]{1,0:T(8,128)(2,1)} %bitcast.39, bf16[64,1024]{1,0:T(8,128)(2,1)} %bitcast.40, bf16[64,1024]{1,0:T(8,128)(2,1)} %bitcast.41), custom_call_target="tpu_custom_call" | custom-call | flops 16777216 | bytes 1048576 | tf_op jit(solution)/shard_map/pallas_call | solution.py:193
  2.3 3.9 %collective-permute-start = (bf16[3,64,1024]{2,1,0:T(8,128)(2,1)}, bf16[3,64,1024]{2,1,0:T(8,128)(2,1)S(1)}, u32[]{:S(2)}, u32[]{:S(2)}) collective-permute-start(bf16[3,64,1024]{2,1,0:T(8,128)(2,1)} %get-tuple-element.11), channel_id=1, source_target_pairs={{0,1},{1,2},{2,3},{3,0},{4,5},{5,6},{6,7},{7,4},{8,9},{9,10},{10,1... | collective-permute-start | bytes 1179656 | tf_op jit(solution)/shard_map/ppermute | solution.py:212
  6.2 3.2 %collective-permute-start.1 = (bf16[3,64,1024]{2,1,0:T(8,128)(2,1)}, bf16[3,64,1024]{2,1,0:T(8,128)(2,1)S(1)}, u32[]{:S(2)}, u32[]{:S(2)}) collective-permute-start(bf16[3,64,1024]{2,1,0:T(8,128)(2,1)} %get-tuple-element.11), channel_id=1, source_target_pairs={{0,3},{1,0},{2,1},{3,2},{4,7},{5,4},{6,5},{7,6},{8,11},{9,8},{10,9... | collective-permute-start | bytes 1179656 | tf_op jit(solution)/shard_map/ppermute | solution.py:213
  9.4 17.3 %all-to-all-start = ((bf16[64,8,128]{2,1,0:T(8,128)(2,1)}), bf16[64,8,128]{2,1,0:T(8,128)(2,1)S(1)}, u32[]{:S(2)}, u32[]{:S(2)}) async-start(bf16[64,8,128]{2,1,0:T(8,128)(2,1)} %bitcast.42), calls=%async_computation | async-start | bytes 262144 | tf_op jit(solution)/shard_map/all_to_all | solution.py:262
  26.7 0.0 copy-start.3
  26.7 0.1 broadcast_in_dim.21
  26.9 0.9 copy-done.3
  27.7 0.1 broadcast_in_dim.26
  27.9 0.0 collective-permute-done
  27.9 2.9 %collective-permute-start.2 = (bf16[2,64,1024]{2,1,0:T(8,128)(2,1)S(1)}, bf16[2,64,1024]{2,1,0:T(8,128)(2,1)S(1)}, u32[]{:S(2)}, u32[]{:S(2)}) collective-permute-start(bf16[2,64,1024]{2,1,0:T(8,128)(2,1)S(1)} %slice.26), channel_id=1, source_target_pairs={{0,1},{1,2},{2,3},{3,0},{4,5},{5,6},{6,7},{7,4},{8,9},{9,10},{10,1... | collective-permute-start | bytes 786440 | tf_op jit(solution)/shard_map/ppermute | solution.py:214
  30.8 0.0 collective-permute-done.1
  30.9 11.0 %all-to-all-done = bf16[64,8,128]{2,1,0:T(8,128)(2,1)S(1)} async-done(((bf16[64,8,128]{2,1,0:T(8,128)(2,1)}), bf16[64,8,128]{2,1,0:T(8,128)(2,1)S(1)}, u32[]{:S(2)}, u32[]{:S(2)}) %all-to-all-start) | async-done | bytes 131104 | tf_op jit(solution)/shard_map/all_to_all | solution.py:262
  41.9 0.8 shard_map.74
  42.8 7.8 %all-to-all-start.1 = ((bf16[8,256,128]{2,1,0:T(8,128)(2,1)}), bf16[8,256,128]{2,1,0:T(8,128)(2,1)S(1)}, u32[]{:S(2)}, u32[]{:S(2)}) async-start(bf16[8,256,128]{2,1,0:T(8,128)(2,1)} %bitcast.10), calls=%async_computation.1 | async-start | bytes 1048576 | tf_op jit(solution)/shard_map/all_to_all | solution.py:273
  50.6 0.0 collective-permute-done.2
  50.6 0.0 copy-start
  50.6 9.3 %all-to-all-done.1 = bf16[8,256,128]{2,1,0:T(8,128)(2,1)S(1)} async-done(((bf16[8,256,128]{2,1,0:T(8,128)(2,1)}), bf16[8,256,128]{2,1,0:T(8,128)(2,1)S(1)}, u32[]{:S(2)}, u32[]{:S(2)}) %all-to-all-start.1) | async-done | bytes 524320 | tf_op jit(solution)/shard_map/all_to_all | solution.py:273
  59.9 0.0 copy-done
  59.9 1.7 %shard_map.75 = bf16[4,256,256]{2,1,0:T(8,128)(2,1)} custom-call(bf16[2,16,64,128]{3,2,1,0:T(8,128)(2,1)S(1)} %bitcast.34, f32[1,1024]{1,0:T(1,128)S(1)} %bitcast.37, bf16[4,2,64,1024]{3,2,1,0:T(8,128)(2,1)S(1)} %bitcast_dynamic-update-slice_fusion.weights_ref), custom_call_target="tpu_custom_call" | custom-call | flops 268435456 | bytes 1048576 | tf_op jit(solution)/shard_map/pallas_call | solution.py:193
  61.6 3.5 %all-to-all-start.2 = ((bf16[4,256,256]{2,1,0:T(8,128)(2,1)}), bf16[4,256,256]{2,1,0:T(8,128)(2,1)S(1)}, u32[]{:S(2)}, u32[]{:S(2)}) async-start(bf16[4,256,256]{2,1,0:T(8,128)(2,1)} %shard_map.75), calls=%async_computation.2 | async-start | bytes 1048576 | tf_op jit(solution)/shard_map/all_to_all | solution.py:285
  65.1 2.6 %collective-permute-start.3 = (bf16[64,1024]{1,0:T(8,128)(2,1)S(1)}, bf16[64,1024]{1,0:T(8,128)(2,1)S(1)}, u32[]{:S(2)}, u32[]{:S(2)}) collective-permute-start(bf16[64,1024]{1,0:T(8,128)(2,1)S(1)} %get-tuple-element.15), channel_id=1, source_target_pairs={{0,3},{1,0},{2,1},{3,2},{4,7},{5,4},{6,5},{7,6},{8,11},{9,8},{10,9... | collective-permute-start | bytes 393224 | tf_op jit(solution)/shard_map/ppermute | solution.py:215
  67.7 4.0 %collective-permute-done.3 = bf16[64,1024]{1,0:T(8,128)(2,1)S(1)} collective-permute-done((bf16[64,1024]{1,0:T(8,128)(2,1)S(1)}, bf16[64,1024]{1,0:T(8,128)(2,1)S(1)}, u32[]{:S(2)}, u32[]{:S(2)}) %collective-permute-start.3) | collective-permute-done | bytes 131104 | tf_op jit(solution)/shard_map/ppermute | solution.py:215
  71.7 2.5 %all-to-all-done.2.hidden_ref = bf16[4,256,256]{2,1,0:T(8,128)(2,1)S(1)} async-done(((bf16[4,256,256]{2,1,0:T(8,128)(2,1)}), bf16[4,256,256]{2,1,0:T(8,128)(2,1)S(1)}, u32[]{:S(2)}, u32[]{:S(2)}) %all-to-all-start.2) | async-done | bytes 524320 | tf_op jit(solution)/shard_map/all_to_all | solution.py:285
  74.3 1.1 %shard_map.76 = bf16[512,128]{1,0:T(8,128)(2,1)} custom-call(bf16[4,256,256]{2,1,0:T(8,128)(2,1)S(1)} %all-to-all-done.2.hidden_ref, bf16[4,64,1024]{2,1,0:T(8,128)(2,1)S(1)} %bitcast_dynamic-update-slice_fusion.3.weights_ref), custom_call_target="tpu_custom_call" | custom-call | flops 134217728 | bytes 1048576 | tf_op jit(solution)/shard_map/pallas_call | solution.py:193
  75.4 0.0 copy-start.2
  75.4 6.5 %all-to-all-start.3 = ((bf16[128,4,128]{2,1,0:T(4,128)(2,1)}), bf16[128,4,128]{2,1,0:T(4,128)(2,1)S(1)}, u32[]{:S(2)}, u32[]{:S(2)}) async-start(bf16[128,4,128]{2,1,0:T(4,128)(2,1)} %bitcast.19), calls=%async_computation.3 | async-start | bytes 262144 | tf_op jit(solution)/shard_map/all_to_all | solution.py:295
  81.8 0.0 copy-start.1
  81.9 0.0 copy-done.2
  81.9 0.7 copy-done.1
  82.5 0.3 shard_map.77
  82.8 17.4 %all-to-all-done.3 = bf16[128,4,128]{2,1,0:T(4,128)(2,1)S(1)} async-done(((bf16[128,4,128]{2,1,0:T(4,128)(2,1)}), bf16[128,4,128]{2,1,0:T(4,128)(2,1)S(1)}, u32[]{:S(2)}, u32[]{:S(2)}) %all-to-all-start.3) | async-done | bytes 131104 | tf_op jit(solution)/shard_map/all_to_all | solution.py:295
  100.2 0.9 shard_map.78
  (9 shorter events, 0.2 us)
Async XLA Ops:
  2.3 25.6 %collective-permute-start = (bf16[3,64,1024]{2,1,0:T(8,128)(2,1)}, bf16[3,64,1024]{2,1,0:T(8,128)(2,1)S(1)}, u32[]{:S(2)}, u32[]{:S(2)}) collective-permute-start(bf16[3,64,1024]{2,1,0:T(8,128)(2,1)} %get-tuple-element.11), channel_id=1, source_target_pairs={{0,1},{1,2},{2,3},{3,0},{4,5},{5,6},{6,7},{7,4},{8,9},{9,10},{10,1... | collective-permute-start | bytes 1179656 | tf_op jit(solution)/shard_map/ppermute | solution.py:212
  6.2 24.6 %collective-permute-start.1 = (bf16[3,64,1024]{2,1,0:T(8,128)(2,1)}, bf16[3,64,1024]{2,1,0:T(8,128)(2,1)S(1)}, u32[]{:S(2)}, u32[]{:S(2)}) collective-permute-start(bf16[3,64,1024]{2,1,0:T(8,128)(2,1)} %get-tuple-element.11), channel_id=1, source_target_pairs={{0,3},{1,0},{2,1},{3,2},{4,7},{5,4},{6,5},{7,6},{8,11},{9,8},{10,9... | collective-permute-start | bytes 1179656 | tf_op jit(solution)/shard_map/ppermute | solution.py:213
  9.4 32.5 %all-to-all-start = ((bf16[64,8,128]{2,1,0:T(8,128)(2,1)}), bf16[64,8,128]{2,1,0:T(8,128)(2,1)S(1)}, u32[]{:S(2)}, u32[]{:S(2)}) async-start(bf16[64,8,128]{2,1,0:T(8,128)(2,1)} %bitcast.42), calls=%async_computation | async-start | bytes 262144 | tf_op jit(solution)/shard_map/all_to_all | solution.py:262
  26.7 1.0 copy-start.3
  27.9 22.7 %collective-permute-start.2 = (bf16[2,64,1024]{2,1,0:T(8,128)(2,1)S(1)}, bf16[2,64,1024]{2,1,0:T(8,128)(2,1)S(1)}, u32[]{:S(2)}, u32[]{:S(2)}) collective-permute-start(bf16[2,64,1024]{2,1,0:T(8,128)(2,1)S(1)} %slice.26), channel_id=1, source_target_pairs={{0,1},{1,2},{2,3},{3,0},{4,5},{5,6},{6,7},{7,4},{8,9},{9,10},{10,1... | collective-permute-start | bytes 786440 | tf_op jit(solution)/shard_map/ppermute | solution.py:214
  42.8 17.1 %all-to-all-start.1 = ((bf16[8,256,128]{2,1,0:T(8,128)(2,1)}), bf16[8,256,128]{2,1,0:T(8,128)(2,1)S(1)}, u32[]{:S(2)}, u32[]{:S(2)}) async-start(bf16[8,256,128]{2,1,0:T(8,128)(2,1)} %bitcast.10), calls=%async_computation.1 | async-start | bytes 1048576 | tf_op jit(solution)/shard_map/all_to_all | solution.py:273
  50.6 9.3 %copy-start = (f32[1024]{0:T(1024)S(1)}, f32[1024]{0:T(1024)}, u32[]{:S(2)}) copy-start(f32[1024]{0:T(1024)} %param.8) | copy-start | bytes 12292
  61.6 12.7 %all-to-all-start.2 = ((bf16[4,256,256]{2,1,0:T(8,128)(2,1)}), bf16[4,256,256]{2,1,0:T(8,128)(2,1)S(1)}, u32[]{:S(2)}, u32[]{:S(2)}) async-start(bf16[4,256,256]{2,1,0:T(8,128)(2,1)} %shard_map.75), calls=%async_computation.2 | async-start | bytes 1048576 | tf_op jit(solution)/shard_map/all_to_all | solution.py:285
  65.1 6.7 %collective-permute-start.3 = (bf16[64,1024]{1,0:T(8,128)(2,1)S(1)}, bf16[64,1024]{1,0:T(8,128)(2,1)S(1)}, u32[]{:S(2)}, u32[]{:S(2)}) collective-permute-start(bf16[64,1024]{1,0:T(8,128)(2,1)S(1)} %get-tuple-element.15), channel_id=1, source_target_pairs={{0,3},{1,0},{2,1},{3,2},{4,7},{5,4},{6,5},{7,6},{8,11},{9,8},{10,9... | collective-permute-start | bytes 393224 | tf_op jit(solution)/shard_map/ppermute | solution.py:215
  75.4 6.5 %copy-start.2 = (s32[4,128]{1,0:T(4,128)S(1)}, s32[4,128]{1,0:T(4,128)}, u32[]{:S(2)}) copy-start(s32[4,128]{1,0:T(4,128)} %get-tuple-element.12.place_ref) | copy-start | bytes 6148
  75.4 24.8 %all-to-all-start.3 = ((bf16[128,4,128]{2,1,0:T(4,128)(2,1)}), bf16[128,4,128]{2,1,0:T(4,128)(2,1)S(1)}, u32[]{:S(2)}, u32[]{:S(2)}) async-start(bf16[128,4,128]{2,1,0:T(4,128)(2,1)} %bitcast.19), calls=%async_computation.3 | async-start | bytes 262144 | tf_op jit(solution)/shard_map/all_to_all | solution.py:295
  81.8 0.7 copy-start.1

commit v3 on v2

--- a/solution.py
+++ b/solution.py
@@ -100,7 +100,8 @@
         copy.wait()
 
 
-def mix_kernel(place_ref, weight_ref, first_ref, rest_ref):
+def mix_kernel(place_ref, weight_ref, gain_ref, first_ref, rest_ref, gain_out_ref):
+    gain_out_ref[...] = gain_ref[...]
     count, toks = first_ref.shape
     lane = iota((count, toks), 0)
     mix = jnp.zeros((count, toks), F32)
@@ -215,12 +216,11 @@
     far_down = lax.ppermute(right[2], TX, after)
     up = jnp.zeros((count, 2) + shard.shape[1:], shard.dtype)
     down = jnp.zeros((count,) + shard.shape[1:], shard.dtype)
-    up, down = set_at(up, shard[:2], me), set_at(down, shard[2], me)
     before, behind, across = (lax.rem(me + hop, count) for hop in (count - 1, 1, count - 2))
-    for piece, source in ((left, before), (right, behind)):
+    for piece, source in ((left, before), (right, behind), (shard, me)):
         up = set_at(up, piece[:2], source)
     up = set_at(up, far_up, across)
-    for piece, source in ((left, before), (right, behind)):
+    for piece, source in ((left, before), (right, behind), (shard, me)):
         down = set_at(down, piece[2], source)
     down = set_at(down, far_down, across)
     return up, down
@@ -273,11 +273,18 @@
     rows = lax.all_to_all(
         spread.reshape(cores * ny, nx * nz * inner, wide), (CORE, TY), 0, 0, tiled=True
     )
+    first, rest, gain = call(
+        mix_kernel,
+        [shape((2 * count, tok_rows), BF16)] * 2 + [shape((1, full), F32)],
+        place,
+        route_weight.astype(F32).T,
+        norm_gain.astype(F32).reshape(1, full),
+    )
     hidden = call(
         up_kernel,
         shape((ny, 2 * group, nx * units), BF16),
         rows.reshape(cores, tp, nz * inner, wide),
-        norm_gain.astype(F32).reshape(1, full),
+        gain,
         w_up,
         flops=1 << 28,
         scratch=(pltpu.VMEM((2 * group, full), F32), pltpu.VMEM((2 * group, full), BF16)),
@@ -294,12 +301,6 @@
 
     back = lax.all_to_all(
         out.reshape(ep * nx, inner, wide), (Z, CORE, TX), 0, 0, tiled=True
-    )
-    first, rest = call(
-        mix_kernel,
-        [shape((2 * count, tok_rows), BF16)] * 2,
-        place,
-        route_weight.astype(F32).T,
     )
     combined = call(
         combine_kernel, shape((width, tok_rows), BF16), back.reshape(count, wide), first, rest

time: 102 us -> 103 us (level)
  blocking collectives: 0 us -> 26.3 us
  waiting for transfers between devices: 44.3 us -> 24.7 us
  starting transfers between devices: 47.6 us -> 41.8 us
    all_to_all x0 -> x1, blocking collectives: none -> 26.3 us  [body(): lax.all_to_all(out.reshape(ep * nx, inner, wide), (Z, CORE, TX), 0, 0, ti...]
    all_to_all x1 -> x0, waiting for transfers between devices: 17.4 us -> none  [body(): lax.all_to_all(out.reshape(ep * nx, inner, wide), (Z, CORE, TX), 0, 0, ti...]
    all_to_all x1, waiting for transfers between devices: 2.54 us -> 9.19 us  [body(): hidden = lax.all_to_all(hidden, TY, 0, 0, tiled=True)]
    all_to_all x1 -> x0, starting transfers between devices: 6.47 us -> none  [body(): lax.all_to_all(out.reshape(ep * nx, inner, wide), (Z, CORE, TX), 0, 0, ti...]
    ppermute x1, waiting for transfers between devices: 4.03 us -> 0.01 us  [gathered(): far_down = lax.ppermute(right[2], TX, after)]
    all_to_all x1, waiting for transfers between devices: 11 us -> 7.13 us  [body(): lax.all_to_all(sent.reshape(nz * nx, cores * inner, wide), (Z, TX), 0, 0,...]
    ppermute x1, starting transfers between devices: 2.62 us -> 4.13 us  [gathered(): far_down = lax.ppermute(right[2], TX, after)]
  transfers between devices with their start and end apart: 8 -> 7, of which waited for: 5 -> 3; matrix products, arithmetic and copies ran while one was open for 0% -> 2% of each run, Pallas kernels for 1% -> 3%
where the time goes in v3:
time: 103 us; the launch traced here: 102 us
  starting transfers between devices  41.8 us (41%)
  blocking collectives  26.3 us (26%)
  waiting for transfers between devices  24.7 us (24%)
  Pallas kernels  6.33 us (6%)
  local copies, waits for them, and re-layouts  2.7 us (3%)
    all_to_all x1, blocking collectives, body(): lax.all_to_all(out.reshape(ep * nx, inner, wide), (Z, CORE, TX), 0, 0, ti...  26.3 us
    all_to_all x1, starting transfers between devices, body(): lax.all_to_all(sent.reshape(nz * nx, cores * inner, wide), (Z, TX), 0, 0,...  17.3 us
    all_to_all x1, waiting for transfers between devices, body(): hidden = lax.all_to_all(hidden, TY, 0, 0, tiled=True)  9.19 us
    all_to_all x1, waiting for transfers between devices, body(): lax.all_to_all(spread.reshape(cores * ny, nx * nz * inner, wide), (CORE,...  8.32 us
    all_to_all x1, starting transfers between devices, body(): lax.all_to_all(spread.reshape(cores * ny, nx * nz * inner, wide), (CORE,...  7.87 us
    all_to_all x1, waiting for transfers between devices, body(): lax.all_to_all(sent.reshape(nz * nx, cores * inner, wide), (Z, TX), 0, 0,...  7.13 us
    pallas_call x6, Pallas kernels, call(): pl.pallas_call(kernel, out_shape=out_shapes, in_specs=[pl.BlockSpec(memor...  6.33 us
    ppermute x1, starting transfers between devices, gathered(): far_down = lax.ppermute(right[2], TX, after)  4.13 us
  transfers between devices with their start and end apart: 7, of which 3 were waited for; matrix products, arithmetic and copies ran while one was open for 2% of the time, Pallas kernels for 3%

profile of v3, /device:TPU:1, one launch (start us, length us, event | category | flops | bytes accessed | tf_op | source)
XLA Modules:
  0.0 102.0 jit_solution(4370899162000841716)
XLA Ops:
  0.0 2.3 %shard_map.73 = (bf16[512,128]{1,0:T(8,128)(2,1)}, s32[4,128]{1,0:T(4,128)}, bf16[3,64,1024]{2,1,0:T(8,128)(2,1)}) custom-call(s32[4,128]{1,0:T(4,128)} %bitcast.45, bf16[64,128]{1,0:T(8,128)(2,1)} %bitcast.44, bf16[64,1024]{1,0:T(8,128)(2,1)} %bitcast.40, bf16[64,1024]{1,0:T(8,128)(2,1)} %bitcast.41, bf16[64,1024]{1,0:T(8,128)(2,1)} %bitcast.42), custom_call_target="tpu_custom_call" | custom-call | flops 16777216 | bytes 1048576 | tf_op jit(solution)/shard_map/pallas_call | solution.py:194
  2.3 3.9 %collective-permute-start = (bf16[3,64,1024]{2,1,0:T(8,128)(2,1)}, bf16[3,64,1024]{2,1,0:T(8,128)(2,1)S(1)}, u32[]{:S(2)}, u32[]{:S(2)}) collective-permute-start(bf16[3,64,1024]{2,1,0:T(8,128)(2,1)} %get-tuple-element.14), channel_id=1, source_target_pairs={{0,1},{1,2},{2,3},{3,0},{4,5},{5,6},{6,7},{7,4},{8,9},{9,10},{10,1... | collective-permute-start | bytes 1179656 | tf_op jit(solution)/shard_map/ppermute | solution.py:213
  6.2 3.2 %collective-permute-start.1 = (bf16[3,64,1024]{2,1,0:T(8,128)(2,1)}, bf16[3,64,1024]{2,1,0:T(8,128)(2,1)S(1)}, u32[]{:S(2)}, u32[]{:S(2)}) collective-permute-start(bf16[3,64,1024]{2,1,0:T(8,128)(2,1)} %get-tuple-element.14), channel_id=1, source_target_pairs={{0,3},{1,0},{2,1},{3,2},{4,7},{5,4},{6,5},{7,6},{8,11},{9,8},{10,9... | collective-permute-start | bytes 1179656 | tf_op jit(solution)/shard_map/ppermute | solution.py:214
  9.4 17.3 %all-to-all-start = ((bf16[64,8,128]{2,1,0:T(8,128)(2,1)}), bf16[64,8,128]{2,1,0:T(8,128)(2,1)S(1)}, u32[]{:S(2)}, u32[]{:S(2)}) async-start(bf16[64,8,128]{2,1,0:T(8,128)(2,1)} %bitcast.43), calls=%async_computation | async-start | bytes 262144 | tf_op jit(solution)/shard_map/all_to_all | solution.py:262
  26.7 0.0 copy-start.2
  26.7 0.0 copy-start
  26.8 0.0 copy-start.1
  26.8 0.6 copy-done.2
  27.4 0.0 copy-done
  27.4 0.0 copy-done.1
  27.4 0.3 shard_map.75
  27.7 0.0 collective-permute-done
  27.7 0.1 broadcast_in_dim.26
  27.8 0.0 collective-permute-done.1
  27.8 4.1 %collective-permute-start.3 = (bf16[64,1024]{1,0:T(8,128)(2,1)S(1)}, bf16[64,1024]{1,0:T(8,128)(2,1)S(1)}, u32[]{:S(2)}, u32[]{:S(2)}) collective-permute-start(bf16[64,1024]{1,0:T(8,128)(2,1)S(1)} %get-tuple-element.17), channel_id=1, source_target_pairs={{0,3},{1,0},{2,1},{3,2},{4,7},{5,4},{6,5},{7,6},{8,11},{9,8},{10,9... | collective-permute-start | bytes 393224 | tf_op jit(solution)/shard_map/ppermute | solution.py:216
  32.0 0.7 slice.26
  32.7 1.9 %collective-permute-start.2 = (bf16[2,64,1024]{2,1,0:T(8,128)(2,1)}, bf16[2,64,1024]{2,1,0:T(8,128)(2,1)}, u32[]{:S(2)}, u32[]{:S(2)}) collective-permute-start(bf16[2,64,1024]{2,1,0:T(8,128)(2,1)} %slice.26), channel_id=1, source_target_pairs={{0,1},{1,2},{2,3},{3,0},{4,5},{5,6},{6,7},{7,4},{8,9},{9,10},{10,1... | collective-permute-start | bytes 786440 | tf_op jit(solution)/shard_map/ppermute | solution.py:215
  34.6 0.1 broadcast_in_dim.21
  34.8 7.1 %all-to-all-done = bf16[64,8,128]{2,1,0:T(8,128)(2,1)S(1)} async-done(((bf16[64,8,128]{2,1,0:T(8,128)(2,1)}), bf16[64,8,128]{2,1,0:T(8,128)(2,1)S(1)}, u32[]{:S(2)}, u32[]{:S(2)}) %all-to-all-start) | async-done | bytes 131104 | tf_op jit(solution)/shard_map/all_to_all | solution.py:262
  41.9 0.8 shard_map.74
  42.8 0.0 copy-start.3
  42.8 7.9 %all-to-all-start.1 = ((bf16[8,256,128]{2,1,0:T(8,128)(2,1)}), bf16[8,256,128]{2,1,0:T(8,128)(2,1)S(1)}, u32[]{:S(2)}, u32[]{:S(2)}) async-start(bf16[8,256,128]{2,1,0:T(8,128)(2,1)} %bitcast.10), calls=%async_computation.1 | async-start | bytes 1048576 | tf_op jit(solution)/shard_map/all_to_all | solution.py:273
  50.7 0.0 copy-done.3
  50.7 0.0 collective-permute-done.2
  50.7 1.0 bitcast_dynamic-update-slice_fusion.weights_ref
  51.7 8.3 %all-to-all-done.1 = bf16[8,256,128]{2,1,0:T(8,128)(2,1)S(1)} async-done(((bf16[8,256,128]{2,1,0:T(8,128)(2,1)}), bf16[8,256,128]{2,1,0:T(8,128)(2,1)S(1)}, u32[]{:S(2)}, u32[]{:S(2)}) %all-to-all-start.1) | async-done | bytes 524320 | tf_op jit(solution)/shard_map/all_to_all | solution.py:273
  60.0 1.7 %shard_map.76 = bf16[4,256,256]{2,1,0:T(8,128)(2,1)} custom-call(bf16[2,16,64,128]{3,2,1,0:T(8,128)(2,1)S(1)} %bitcast.34, f32[1,1024]{1,0:T(1,128)S(1)} %get-tuple-element.13.gain_ref, bf16[4,2,64,1024]{3,2,1,0:T(8,128)(2,1)S(1)} %bitcast_dynamic-update-slice_fusion.weights_ref), custom_call_target="tpu_custom_call" | custom-call | flops 268435456 | bytes 1048576 | tf_op jit(solution)/shard_map/pallas_call | solution.py:194
  61.7 3.5 %all-to-all-start.2 = ((bf16[4,256,256]{2,1,0:T(8,128)(2,1)}), bf16[4,256,256]{2,1,0:T(8,128)(2,1)S(1)}, u32[]{:S(2)}, u32[]{:S(2)}) async-start(bf16[4,256,256]{2,1,0:T(8,128)(2,1)} %shard_map.76), calls=%async_computation.2 | async-start | bytes 1048576 | tf_op jit(solution)/shard_map/all_to_all | solution.py:292
  65.2 0.0 collective-permute-done.3
  65.2 9.2 %all-to-all-done.2.hidden_ref = bf16[4,256,256]{2,1,0:T(8,128)(2,1)S(1)} async-done(((bf16[4,256,256]{2,1,0:T(8,128)(2,1)}), bf16[4,256,256]{2,1,0:T(8,128)(2,1)S(1)}, u32[]{:S(2)}, u32[]{:S(2)}) %all-to-all-start.2) | async-done | bytes 524320 | tf_op jit(solution)/shard_map/all_to_all | solution.py:292
  74.4 0.4 shard_map.77
  74.8 26.3 %all_to_all.20 = bf16[128,4,128]{2,1,0:T(4,128)(2,1)S(1)} all-to-all(bf16[128,4,128]{2,1,0:T(4,128)(2,1)S(1)} %bitcast.36), channel_id=1, replica_groups=mesh['z'=16,'core'=2,'ty'=4,'tx'=4] {'z','core','tx'}, dimensions={0} | all-to-all | bytes 262144 | tf_op jit(solution)/shard_map/all_to_all | solution.py:302
  101.1 0.9 shard_map.78
  (7 shorter events, 0.1 us)
Async XLA Ops:
  2.3 25.4 %collective-permute-start = (bf16[3,64,1024]{2,1,0:T(8,128)(2,1)}, bf16[3,64,1024]{2,1,0:T(8,128)(2,1)S(1)}, u32[]{:S(2)}, u32[]{:S(2)}) collective-permute-start(bf16[3,64,1024]{2,1,0:T(8,128)(2,1)} %get-tuple-element.14), channel_id=1, source_target_pairs={{0,1},{1,2},{2,3},{3,0},{4,5},{5,6},{6,7},{7,4},{8,9},{9,10},{10,1... | collective-permute-start | bytes 1179656 | tf_op jit(solution)/shard_map/ppermute | solution.py:213
  6.2 21.6 %collective-permute-start.1 = (bf16[3,64,1024]{2,1,0:T(8,128)(2,1)}, bf16[3,64,1024]{2,1,0:T(8,128)(2,1)S(1)}, u32[]{:S(2)}, u32[]{:S(2)}) collective-permute-start(bf16[3,64,1024]{2,1,0:T(8,128)(2,1)} %get-tuple-element.14), channel_id=1, source_target_pairs={{0,3},{1,0},{2,1},{3,2},{4,7},{5,4},{6,5},{7,6},{8,11},{9,8},{10,9... | collective-permute-start | bytes 1179656 | tf_op jit(solution)/shard_map/ppermute | solution.py:214
  9.4 32.5 %all-to-all-start = ((bf16[64,8,128]{2,1,0:T(8,128)(2,1)}), bf16[64,8,128]{2,1,0:T(8,128)(2,1)S(1)}, u32[]{:S(2)}, u32[]{:S(2)}) async-start(bf16[64,8,128]{2,1,0:T(8,128)(2,1)} %bitcast.43), calls=%async_computation | async-start | bytes 262144 | tf_op jit(solution)/shard_map/all_to_all | solution.py:262
  26.7 0.7 copy-start.2
  26.7 0.7 copy-start
  26.8 0.7 copy-start.1
  27.8 37.3 %collective-permute-start.3 = (bf16[64,1024]{1,0:T(8,128)(2,1)S(1)}, bf16[64,1024]{1,0:T(8,128)(2,1)S(1)}, u32[]{:S(2)}, u32[]{:S(2)}) collective-permute-start(bf16[64,1024]{1,0:T(8,128)(2,1)S(1)} %get-tuple-element.17), channel_id=1, source_target_pairs={{0,3},{1,0},{2,1},{3,2},{4,7},{5,4},{6,5},{7,6},{8,11},{9,8},{10,9... | collective-permute-start | bytes 393224 | tf_op jit(solution)/shard_map/ppermute | solution.py:216
  32.7 18.0 %collective-permute-start.2 = (bf16[2,64,1024]{2,1,0:T(8,128)(2,1)}, bf16[2,64,1024]{2,1,0:T(8,128)(2,1)}, u32[]{:S(2)}, u32[]{:S(2)}) collective-permute-start(bf16[2,64,1024]{2,1,0:T(8,128)(2,1)} %slice.26), channel_id=1, source_target_pairs={{0,1},{1,2},{2,3},{3,0},{4,5},{5,6},{6,7},{7,4},{8,9},{9,10},{10,1... | collective-permute-start | bytes 786440 | tf_op jit(solution)/shard_map/ppermute | solution.py:215
  42.8 7.9 %copy-start.3 = (bf16[3,64,1024]{2,1,0:T(8,128)(2,1)S(1)}, bf16[3,64,1024]{2,1,0:T(8,128)(2,1)}, u32[]{:S(2)}) copy-start(bf16[3,64,1024]{2,1,0:T(8,128)(2,1)} %get-tuple-element.14) | copy-start | bytes 1179652
  42.8 17.2 %all-to-all-start.1 = ((bf16[8,256,128]{2,1,0:T(8,128)(2,1)}), bf16[8,256,128]{2,1,0:T(8,128)(2,1)S(1)}, u32[]{:S(2)}, u32[]{:S(2)}) async-start(bf16[8,256,128]{2,1,0:T(8,128)(2,1)} %bitcast.10), calls=%async_computation.1 | async-start | bytes 1048576 | tf_op jit(solution)/shard_map/all_to_all | solution.py:273
  61.7 12.7 %all-to-all-start.2 = ((bf16[4,256,256]{2,1,0:T(8,128)(2,1)}), bf16[4,256,256]{2,1,0:T(8,128)(2,1)S(1)}, u32[]{:S(2)}, u32[]{:S(2)}) async-start(bf16[4,256,256]{2,1,0:T(8,128)(2,1)} %shard_map.76), calls=%async_computation.2 | async-start | bytes 1048576 | tf_op jit(solution)/shard_map/all_to_all | solution.py:292

commit v4 on v3

--- a/solution.py
+++ b/solution.py
@@ -54,11 +54,12 @@
 
 def prep_kernel(
     sizes, ids_hbm, tokens_hbm, gate_hbm, up_hbm, down_hbm, sent_ref, place_ref, shard_ref,
-    ids_ref, tokens_ref, sems
+    pair_ref, ids_ref, tokens_ref, sems
 ):
     nz, cores, nx = sizes
     small = [(ids_hbm, ids_ref), (tokens_hbm, tokens_ref)]
     large = [(w, shard_ref.at[i]) for i, w in enumerate((gate_hbm, up_hbm, down_hbm))]
+    large += [(w, pair_ref.at[i]) for i, w in enumerate((gate_hbm, up_hbm))]
     copies = [pltpu.make_async_copy(a, b, sems.at[i]) for i, (a, b) in enumerate(small + large)]
     for copy in copies:
         copy.start()
@@ -206,13 +207,15 @@
     return lax.dynamic_update_slice_in_dim(whole, piece[None], index, 0)
 
 
-def gathered(shard):
+def gathered(shard, pair):
     count = lax.axis_size(TX)
     me = lax.axis_index(TX)
-    near, after = ([(i, (i + hop) % count) for i in range(count)] for hop in (1, count - 1))
+    near, far, after = (
+        [(i, (i + hop) % count) for i in range(count)] for hop in (1, count - 2, count - 1)
+    )
+    right = lax.ppermute(shard, TX, after)
+    far_up = lax.ppermute(pair, TX, far)
     left = lax.ppermute(shard, TX, near)
-    right = lax.ppermute(shard, TX, after)
-    far_up = lax.ppermute(left[:2], TX, near)
     far_down = lax.ppermute(right[2], TX, after)
     up = jnp.zeros((count, 2) + shard.shape[1:], shard.dtype)
     down = jnp.zeros((count,) + shard.shape[1:], shard.dtype)
@@ -220,7 +223,7 @@
     for piece, source in ((left, before), (right, behind), (shard, me)):
         up = set_at(up, piece[:2], source)
     up = set_at(up, far_up, across)
-    for piece, source in ((left, before), (right, behind), (shard, me)):
+    for piece, source in ((right, behind), (left, before), (shard, me)):
         down = set_at(down, piece[2], source)
     down = set_at(down, far_down, across)
     return up, down
@@ -239,12 +242,13 @@
     group = count // nx
     shape = jax.ShapeDtypeStruct
 
-    sent, place, shard = call(
+    sent, place, shard, pair = call(
         functools.partial(prep_kernel, (nz, cores, nx)),
         [
             shape((count, wide), BF16),
             shape((top, tok_rows), I32),
             shape((3, units, full), BF16),
+            shape((2, units, full), BF16),
         ],
         expert_ids.T,
         tokens.T,
@@ -254,7 +258,7 @@
         scratch=(
             pltpu.VMEM((top, tok_rows), I32),
             pltpu.VMEM((width, tok_rows), BF16),
-            pltpu.SemaphoreType.DMA((5,)),
+            pltpu.SemaphoreType.DMA((7,)),
         ),
         space=pltpu.HBM,
         vmem=62,
@@ -262,7 +266,7 @@
     got = lax.all_to_all(
         sent.reshape(nz * nx, cores * inner, wide), (Z, TX), 0, 0, tiled=True
     )
-    w_up, w_down = gathered(shard)
+    w_up, w_down = gathered(shard, pair)
 
     spread = call(
         spread_kernel,

time: 103 us -> 104 us (level)
  local copies, waits for them, and re-layouts: 2.7 us -> 5.5 us
  blocking collectives: 26.3 us -> 24.1 us
  starting transfers between devices: 41.8 us -> 43.5 us
  waiting for transfers between devices: 24.7 us -> 23.6 us
    all_to_all x1, blocking collectives: 26.3 us -> 24.1 us  [body(): lax.all_to_all(out.reshape(ep * nx, inner, wide), (Z, CORE, TX), 0, 0, ti...]
    ppermute x1, starting transfers between devices: 3.19 us -> 5.2 us  [gathered(): right = lax.ppermute(shard, TX, after)]
    ppermute x1, starting transfers between devices: 3.94 us -> 1.92 us  [gathered(): left = lax.ppermute(shard, TX, near)]
    unnamed x8 -> x12, local copies, waits for them, and re-layouts: 0.69 us -> 2.62 us
    ppermute x1, starting transfers between devices: 1.91 us -> 3.63 us  [gathered(): far_up = lax.ppermute(pair, TX, far)]
  transfers between devices with their start and end apart: 7 -> 7, of which waited for: 3 -> 3; matrix products, arithmetic and copies ran while one was open for 2% -> 3% of each run, Pallas kernels for 3% -> 3%
where the time goes in v4:
time: 104 us; the launch traced here: 103 us
  starting transfers between devices  43.5 us (42%)
  blocking collectives  24.1 us (23%)
  waiting for transfers between devices  23.6 us (23%)
  Pallas kernels  6.47 us (6%)
  local copies, waits for them, and re-layouts  5.5 us (5%)
    all_to_all x1, blocking collectives, body(): lax.all_to_all(out.reshape(ep * nx, inner, wide), (Z, CORE, TX), 0, 0, ti...  24.1 us
    all_to_all x1, starting transfers between devices, body(): lax.all_to_all(sent.reshape(nz * nx, cores * inner, wide), (Z, TX), 0, 0,...  17.1 us
    all_to_all x1, waiting for transfers between devices, body(): lax.all_to_all(spread.reshape(cores * ny, nx * nz * inner, wide), (CORE,...  8.33 us
    all_to_all x1, waiting for transfers between devices, body(): hidden = lax.all_to_all(hidden, TY, 0, 0, tiled=True)  8.29 us
    all_to_all x1, starting transfers between devices, body(): lax.all_to_all(spread.reshape(cores * ny, nx * nz * inner, wide), (CORE,...  8.06 us
    all_to_all x1, waiting for transfers between devices, body(): lax.all_to_all(sent.reshape(nz * nx, cores * inner, wide), (Z, TX), 0, 0,...  6.95 us
    pallas_call x6, Pallas kernels, call(): pl.pallas_call(kernel, out_shape=out_shapes, in_specs=[pl.BlockSpec(memor...  6.47 us
    ppermute x1, starting transfers between devices, gathered(): right = lax.ppermute(shard, TX, after)  5.2 us
  transfers between devices with their start and end apart: 7, of which 3 were waited for; matrix products, arithmetic and copies ran while one was open for 3% of the time, Pallas kernels for 3%

profile of v4, /device:TPU:1, one launch (start us, length us, event | category | flops | bytes accessed | tf_op | source)
XLA Modules:
  0.0 103.3 jit_solution(3327216098234634903)
XLA Ops:
  0.0 2.4 %shard_map.73 = (bf16[512,128]{1,0:T(8,128)(2,1)}, s32[4,128]{1,0:T(4,128)}, bf16[3,64,1024]{2,1,0:T(8,128)(2,1)}, bf16[2,64,1024]{2,1,0:T(8,128)(2,1)}) custom-call(s32[4,128]{1,0:T(4,128)} %bitcast.47, bf16[64,128]{1,0:T(8,128)(2,1)} %bitcast.46, bf16[64,1024]{1,0:T(8,128)(2,1)} %bitcast.42, bf16[64,1024]{1,0:T(8,128)(2,1)} %bitcast.43, ...), custom_call_target="tpu_custom_call" | custom-call | flops 16777216 | bytes 1048576 | tf_op jit(solution)/shard_map/pallas_call | solution.py:195
  2.4 5.2 %collective-permute-start.1 = (bf16[3,64,1024]{2,1,0:T(8,128)(2,1)}, bf16[3,64,1024]{2,1,0:T(8,128)(2,1)S(1)}, u32[]{:S(2)}, u32[]{:S(2)}) collective-permute-start(bf16[3,64,1024]{2,1,0:T(8,128)(2,1)} %get-tuple-element.15), channel_id=1, source_target_pairs={{0,3},{1,0},{2,1},{3,2},{4,7},{5,4},{6,5},{7,6},{8,11},{9,8},{10,9... | collective-permute-start | bytes 1179656 | tf_op jit(solution)/shard_map/ppermute | solution.py:216
  7.6 1.9 %collective-permute-start = (bf16[3,64,1024]{2,1,0:T(8,128)(2,1)}, bf16[3,64,1024]{2,1,0:T(8,128)(2,1)S(1)}, u32[]{:S(2)}, u32[]{:S(2)}) collective-permute-start(bf16[3,64,1024]{2,1,0:T(8,128)(2,1)} %get-tuple-element.15), channel_id=1, source_target_pairs={{0,1},{1,2},{2,3},{3,0},{4,5},{5,6},{6,7},{7,4},{8,9},{9,10},{10,1... | collective-permute-start | bytes 1179656 | tf_op jit(solution)/shard_map/ppermute | solution.py:218
  9.5 3.6 %collective-permute-start.2 = (bf16[2,64,1024]{2,1,0:T(8,128)(2,1)}, bf16[2,64,1024]{2,1,0:T(8,128)(2,1)}, u32[]{:S(2)}, u32[]{:S(2)}) collective-permute-start(bf16[2,64,1024]{2,1,0:T(8,128)(2,1)} %get-tuple-element.16), channel_id=1, source_target_pairs={{0,2},{1,3},{2,0},{3,1},{4,6},{5,7},{6,4},{7,5},{8,10},{9,11},{10,... | collective-permute-start | bytes 786440 | tf_op jit(solution)/shard_map/ppermute | solution.py:217
  13.2 17.1 %all-to-all-start = ((bf16[64,8,128]{2,1,0:T(8,128)(2,1)}), bf16[64,8,128]{2,1,0:T(8,128)(2,1)S(1)}, u32[]{:S(2)}, u32[]{:S(2)}) async-start(bf16[64,8,128]{2,1,0:T(8,128)(2,1)} %bitcast.45), calls=%async_computation | async-start | bytes 262144 | tf_op jit(solution)/shard_map/all_to_all | solution.py:266
  30.3 0.0 copy-start.2
  30.3 0.0 copy-start
  30.3 0.0 copy-start.1
  30.3 0.6 copy-done.2
  31.0 0.0 copy-done
  31.0 0.0 copy-done.1
  31.0 0.3 shard_map.75
  31.3 0.0 collective-permute-done.1
  31.3 0.0 copy-start.4
  31.3 0.1 broadcast_in_dim.26
  31.3 0.7 slice_bitcast_fusion.2
  32.1 0.0 copy-done.4
  32.1 4.1 %collective-permute-start.3 = (bf16[64,1024]{1,0:T(8,128)(2,1)}, bf16[64,1024]{1,0:T(8,128)(2,1)}, u32[]{:S(2)}, u32[]{:S(2)}) collective-permute-start(bf16[64,1024]{1,0:T(8,128)(2,1)} %get-tuple-element.19), channel_id=1, source_target_pairs={{0,3},{1,0},{2,1},{3,2},{4,7},{5,4},{6,5},{7,6},{8,11},{9,8},{10,9... | collective-permute-start | bytes 393224 | tf_op jit(solution)/shard_map/ppermute | solution.py:219
  36.2 0.0 collective-permute-done
  36.2 0.1 broadcast_in_dim.21
  36.3 0.0 copy-start.5
  36.4 1.0 copy-done.5
  37.3 0.0 copy-start.3
  37.4 1.0 copy-done.3
  38.3 6.9 %all-to-all-done = bf16[64,8,128]{2,1,0:T(8,128)(2,1)S(1)} async-done(((bf16[64,8,128]{2,1,0:T(8,128)(2,1)}), bf16[64,8,128]{2,1,0:T(8,128)(2,1)S(1)}, u32[]{:S(2)}, u32[]{:S(2)}) %all-to-all-start) | async-done | bytes 131104 | tf_op jit(solution)/shard_map/all_to_all | solution.py:266
  45.3 0.8 shard_map.74
  46.1 8.1 %all-to-all-start.1 = ((bf16[8,256,128]{2,1,0:T(8,128)(2,1)}), bf16[8,256,128]{2,1,0:T(8,128)(2,1)S(1)}, u32[]{:S(2)}, u32[]{:S(2)}) async-start(bf16[8,256,128]{2,1,0:T(8,128)(2,1)} %bitcast.10), calls=%async_computation.1 | async-start | bytes 1048576 | tf_op jit(solution)/shard_map/all_to_all | solution.py:277
  54.2 0.0 collective-permute-done.2
  54.2 1.0 bitcast_dynamic-update-slice_fusion.weights_ref
  55.2 8.3 %all-to-all-done.1 = bf16[8,256,128]{2,1,0:T(8,128)(2,1)S(1)} async-done(((bf16[8,256,128]{2,1,0:T(8,128)(2,1)}), bf16[8,256,128]{2,1,0:T(8,128)(2,1)S(1)}, u32[]{:S(2)}, u32[]{:S(2)}) %all-to-all-start.1) | async-done | bytes 524320 | tf_op jit(solution)/shard_map/all_to_all | solution.py:277
  63.5 1.7 %shard_map.76 = bf16[4,256,256]{2,1,0:T(8,128)(2,1)} custom-call(bf16[2,16,64,128]{3,2,1,0:T(8,128)(2,1)S(1)} %bitcast.36, f32[1,1024]{1,0:T(1,128)S(1)} %get-tuple-element.14.gain_ref, bf16[4,2,64,1024]{3,2,1,0:T(8,128)(2,1)S(1)} %bitcast_dynamic-update-slice_fusion.weights_ref), custom_call_target="tpu_custom_call" | custom-call | flops 268435456 | bytes 1048576 | tf_op jit(solution)/shard_map/pallas_call | solution.py:195
  65.2 3.5 %all-to-all-start.2 = ((bf16[4,256,256]{2,1,0:T(8,128)(2,1)}), bf16[4,256,256]{2,1,0:T(8,128)(2,1)S(1)}, u32[]{:S(2)}, u32[]{:S(2)}) async-start(bf16[4,256,256]{2,1,0:T(8,128)(2,1)} %shard_map.76), calls=%async_computation.2 | async-start | bytes 1048576 | tf_op jit(solution)/shard_map/all_to_all | solution.py:296
  68.7 0.0 collective-permute-done.3
  68.7 0.9 bitcast_dynamic-update-slice_fusion.2.weights_ref
  69.6 8.3 %all-to-all-done.2.hidden_ref = bf16[4,256,256]{2,1,0:T(8,128)(2,1)S(1)} async-done(((bf16[4,256,256]{2,1,0:T(8,128)(2,1)}), bf16[4,256,256]{2,1,0:T(8,128)(2,1)S(1)}, u32[]{:S(2)}, u32[]{:S(2)}) %all-to-all-start.2) | async-done | bytes 524320 | tf_op jit(solution)/shard_map/all_to_all | solution.py:296
  77.9 0.4 shard_map.77
  78.3 24.1 %all_to_all.20 = bf16[128,4,128]{2,1,0:T(4,128)(2,1)S(1)} all-to-all(bf16[128,4,128]{2,1,0:T(4,128)(2,1)S(1)} %bitcast.38), channel_id=1, replica_groups=mesh['z'=16,'core'=2,'ty'=4,'tx'=4] {'z','core','tx'}, dimensions={0} | all-to-all | bytes 262144 | tf_op jit(solution)/shard_map/all_to_all | solution.py:306
  102.4 0.9 shard_map.78
  (5 shorter events, 0.1 us)
Async XLA Ops:
  2.4 28.9 %collective-permute-start.1 = (bf16[3,64,1024]{2,1,0:T(8,128)(2,1)}, bf16[3,64,1024]{2,1,0:T(8,128)(2,1)S(1)}, u32[]{:S(2)}, u32[]{:S(2)}) collective-permute-start(bf16[3,64,1024]{2,1,0:T(8,128)(2,1)} %get-tuple-element.15), channel_id=1, source_target_pairs={{0,3},{1,0},{2,1},{3,2},{4,7},{5,4},{6,5},{7,6},{8,11},{9,8},{10,9... | collective-permute-start | bytes 1179656 | tf_op jit(solution)/shard_map/ppermute | solution.py:216
  7.6 28.6 %collective-permute-start = (bf16[3,64,1024]{2,1,0:T(8,128)(2,1)}, bf16[3,64,1024]{2,1,0:T(8,128)(2,1)S(1)}, u32[]{:S(2)}, u32[]{:S(2)}) collective-permute-start(bf16[3,64,1024]{2,1,0:T(8,128)(2,1)} %get-tuple-element.15), channel_id=1, source_target_pairs={{0,1},{1,2},{2,3},{3,0},{4,5},{5,6},{6,7},{7,4},{8,9},{9,10},{10,1... | collective-permute-start | bytes 1179656 | tf_op jit(solution)/shard_map/ppermute | solution.py:218
  9.5 44.7 %collective-permute-start.2 = (bf16[2,64,1024]{2,1,0:T(8,128)(2,1)}, bf16[2,64,1024]{2,1,0:T(8,128)(2,1)}, u32[]{:S(2)}, u32[]{:S(2)}) collective-permute-start(bf16[2,64,1024]{2,1,0:T(8,128)(2,1)} %get-tuple-element.16), channel_id=1, source_target_pairs={{0,2},{1,3},{2,0},{3,1},{4,6},{5,7},{6,4},{7,5},{8,10},{9,11},{10,... | collective-permute-start | bytes 786440 | tf_op jit(solution)/shard_map/ppermute | solution.py:217
  13.2 32.1 %all-to-all-start = ((bf16[64,8,128]{2,1,0:T(8,128)(2,1)}), bf16[64,8,128]{2,1,0:T(8,128)(2,1)S(1)}, u32[]{:S(2)}, u32[]{:S(2)}) async-start(bf16[64,8,128]{2,1,0:T(8,128)(2,1)} %bitcast.45), calls=%async_computation | async-start | bytes 262144 | tf_op jit(solution)/shard_map/all_to_all | solution.py:266
  30.3 0.7 copy-start.2
  30.3 0.7 copy-start
  30.3 0.7 copy-start.1
  31.3 0.8 copy-start.4
  32.1 36.7 %collective-permute-start.3 = (bf16[64,1024]{1,0:T(8,128)(2,1)}, bf16[64,1024]{1,0:T(8,128)(2,1)}, u32[]{:S(2)}, u32[]{:S(2)}) collective-permute-start(bf16[64,1024]{1,0:T(8,128)(2,1)} %get-tuple-element.19), channel_id=1, source_target_pairs={{0,3},{1,0},{2,1},{3,2},{4,7},{5,4},{6,5},{7,6},{8,11},{9,8},{10,9... | collective-permute-start | bytes 393224 | tf_op jit(solution)/shard_map/ppermute | solution.py:219
  36.3 1.0 copy-start.5
  37.3 1.0 copy-start.3
  46.1 17.4 %all-to-all-start.1 = ((bf16[8,256,128]{2,1,0:T(8,128)(2,1)}), bf16[8,256,128]{2,1,0:T(8,128)(2,1)S(1)}, u32[]{:S(2)}, u32[]{:S(2)}) async-start(bf16[8,256,128]{2,1,0:T(8,128)(2,1)} %bitcast.10), calls=%async_computation.1 | async-start | bytes 1048576 | tf_op jit(solution)/shard_map/all_to_all | solution.py:277
  65.2 12.7 %all-to-all-start.2 = ((bf16[4,256,256]{2,1,0:T(8,128)(2,1)}), bf16[4,256,256]{2,1,0:T(8,128)(2,1)S(1)}, u32[]{:S(2)}, u32[]{:S(2)}) async-start(bf16[4,256,256]{2,1,0:T(8,128)(2,1)} %shard_map.76), calls=%async_computation.2 | async-start | bytes 1048576 | tf_op jit(solution)/shard_map/all_to_all | solution.py:296

commit v5 on v4

--- a/solution.py
+++ b/solution.py
@@ -54,12 +54,12 @@
 
 def prep_kernel(
     sizes, ids_hbm, tokens_hbm, gate_hbm, up_hbm, down_hbm, sent_ref, place_ref, shard_ref,
-    pair_ref, ids_ref, tokens_ref, sems
+    gate_ref, ids_ref, tokens_ref, sems
 ):
     nz, cores, nx = sizes
     small = [(ids_hbm, ids_ref), (tokens_hbm, tokens_ref)]
     large = [(w, shard_ref.at[i]) for i, w in enumerate((gate_hbm, up_hbm, down_hbm))]
-    large += [(w, pair_ref.at[i]) for i, w in enumerate((gate_hbm, up_hbm))]
+    large += [(gate_hbm, gate_ref)]
     copies = [pltpu.make_async_copy(a, b, sems.at[i]) for i, (a, b) in enumerate(small + large)]
     for copy in copies:
         copy.start()
@@ -207,22 +207,24 @@
     return lax.dynamic_update_slice_in_dim(whole, piece[None], index, 0)
 
 
-def gathered(shard, pair):
+def gathered(shard, gate):
     count = lax.axis_size(TX)
     me = lax.axis_index(TX)
     near, far, after = (
         [(i, (i + hop) % count) for i in range(count)] for hop in (1, count - 2, count - 1)
     )
     right = lax.ppermute(shard, TX, after)
-    far_up = lax.ppermute(pair, TX, far)
+    far_gate = lax.ppermute(gate, TX, far)
     left = lax.ppermute(shard, TX, near)
-    far_down = lax.ppermute(right[2], TX, after)
+    far_up = lax.ppermute(right[1], TX, after)
+    far_down = lax.ppermute(left[2], TX, near)
     up = jnp.zeros((count, 2) + shard.shape[1:], shard.dtype)
     down = jnp.zeros((count,) + shard.shape[1:], shard.dtype)
     before, behind, across = (lax.rem(me + hop, count) for hop in (count - 1, 1, count - 2))
-    for piece, source in ((left, before), (right, behind), (shard, me)):
+    for piece, source in ((right, behind), (left, before), (shard, me)):
         up = set_at(up, piece[:2], source)
-    up = set_at(up, far_up, across)
+    for half, piece in enumerate((far_gate, far_up)):
+        up = lax.dynamic_update_slice(up, piece[None, None], (across, half, 0, 0))
     for piece, source in ((right, behind), (left, before), (shard, me)):
         down = set_at(down, piece[2], source)
     down = set_at(down, far_down, across)
@@ -242,13 +244,13 @@
     group = count // nx
     shape = jax.ShapeDtypeStruct
 
-    sent, place, shard, pair = call(
+    sent, place, shard, gate = call(
         functools.partial(prep_kernel, (nz, cores, nx)),
         [
             shape((count, wide), BF16),
             shape((top, tok_rows), I32),
             shape((3, units, full), BF16),
-            shape((2, units, full), BF16),
+            shape((units, full), BF16),
         ],
         expert_ids.T,
         tokens.T,
@@ -258,7 +260,7 @@
         scratch=(
             pltpu.VMEM((top, tok_rows), I32),
             pltpu.VMEM((width, tok_rows), BF16),
-            pltpu.SemaphoreType.DMA((7,)),
+            pltpu.SemaphoreType.DMA((6,)),
         ),
         space=pltpu.HBM,
         vmem=62,
@@ -266,7 +268,7 @@
     got = lax.all_to_all(
         sent.reshape(nz * nx, cores * inner, wide), (Z, TX), 0, 0, tiled=True
     )
-    w_up, w_down = gathered(shard, pair)
+    w_up, w_down = gathered(shard, gate)
 
     spread = call(
         spread_kernel,

time: 104 us -> 107 us (1.029)
  blocking collectives: 24.1 us -> 26.8 us
  local copies, waits for them, and re-layouts: 5.5 us -> 2.89 us
  starting transfers between devices: 43.5 us -> 45.4 us
    all_to_all x1, blocking collectives: 24.1 us -> 26.8 us  [body(): lax.all_to_all(out.reshape(ep * nx, inner, wide), (Z, CORE, TX), 0, 0, ti...]
    ppermute x2 -> x3, starting transfers between devices: 7.75 us -> 9.68 us  [the longest x1 4.13 us: gathered(): far_up = lax.ppermute(right[1], TX, after)]
    dynamic_update_slice x7 -> x6, local copies, waits for them, and re-layouts: 1.99 us -> 0.12 us  [set_at(): return lax.dynamic_update_slice_in_dim(whole, piece[None], index, 0)]
    unnamed x12 -> x8, local copies, waits for them, and re-layouts: 2.62 us -> 1.65 us
  transfers between devices with their start and end apart: 7 -> 8, of which waited for: 3 -> 3; matrix products, arithmetic and copies ran while one was open for 3% -> 1% of each run, Pallas kernels for 3% -> 3%
where the time goes in v5:
time: 107 us; the launch traced here: 106 us
  starting transfers between devices  45.4 us (42%)
  blocking collectives  26.8 us (25%)
  waiting for transfers between devices  24.2 us (23%)
  Pallas kernels  6.4 us (6%)
  local copies, waits for them, and re-layouts  2.89 us (3%)
    all_to_all x1, blocking collectives, body(): lax.all_to_all(out.reshape(ep * nx, inner, wide), (Z, CORE, TX), 0, 0, ti...  26.8 us
    all_to_all x1, starting transfers between devices, body(): lax.all_to_all(sent.reshape(nz * nx, cores * inner, wide), (Z, TX), 0, 0,...  17.1 us
    all_to_all x1, waiting for transfers between devices, body(): hidden = lax.all_to_all(hidden, TY, 0, 0, tiled=True)  9.19 us
    all_to_all x1, waiting for transfers between devices, body(): lax.all_to_all(spread.reshape(cores * ny, nx * nz * inner, wide), (CORE,...  8.38 us
    all_to_all x1, starting transfers between devices, body(): lax.all_to_all(spread.reshape(cores * ny, nx * nz * inner, wide), (CORE,...  8.05 us
    all_to_all x1, waiting for transfers between devices, body(): lax.all_to_all(sent.reshape(nz * nx, cores * inner, wide), (Z, TX), 0, 0,...  6.65 us
    pallas_call x6, Pallas kernels, call(): pl.pallas_call(kernel, out_shape=out_shapes, in_specs=[pl.BlockSpec(memor...  6.4 us
    ppermute x1, starting transfers between devices, gathered(): right = lax.ppermute(shard, TX, after)  5.2 us
  transfers between devices with their start and end apart: 8, of which 3 were waited for; matrix products, arithmetic and copies ran while one was open for 1% of the time, Pallas kernels for 3%

profile of v5, /device:TPU:1, one launch (start us, length us, event | category | flops | bytes accessed | tf_op | source)
XLA Modules:
  0.0 105.9 jit_solution(8974988831261616677)
XLA Ops:
  0.0 2.3 %shard_map.73 = (bf16[512,128]{1,0:T(8,128)(2,1)}, s32[4,128]{1,0:T(4,128)}, bf16[3,64,1024]{2,1,0:T(8,128)(2,1)}, bf16[64,1024]{1,0:T(8,128)(2,1)}) custom-call(s32[4,128]{1,0:T(4,128)} %bitcast.51, bf16[64,128]{1,0:T(8,128)(2,1)} %bitcast.50, bf16[64,1024]{1,0:T(8,128)(2,1)} %bitcast.46, bf16[64,1024]{1,0:T(8,128)(2,1)} %bitcast.47, bf16[64,1024]{1,0:T(8,128)(2,1)} %bitcast.48), custom_call_target="tpu_custom_call" | custom-call | flops 16777216 | bytes 1048576 | tf_op jit(solution)/shard_map/pallas_call | solution.py:195
  2.3 5.2 %collective-permute-start = (bf16[3,64,1024]{2,1,0:T(8,128)(2,1)}, bf16[3,64,1024]{2,1,0:T(8,128)(2,1)S(1)}, u32[]{:S(2)}, u32[]{:S(2)}) collective-permute-start(bf16[3,64,1024]{2,1,0:T(8,128)(2,1)} %get-tuple-element.15), channel_id=1, source_target_pairs={{0,3},{1,0},{2,1},{3,2},{4,7},{5,4},{6,5},{7,6},{8,11},{9,8},{10,9... | collective-permute-start | bytes 1179656 | tf_op jit(solution)/shard_map/ppermute | solution.py:216
  7.5 1.9 %collective-permute-start.1 = (bf16[3,64,1024]{2,1,0:T(8,128)(2,1)}, bf16[3,64,1024]{2,1,0:T(8,128)(2,1)S(1)}, u32[]{:S(2)}, u32[]{:S(2)}) collective-permute-start(bf16[3,64,1024]{2,1,0:T(8,128)(2,1)} %get-tuple-element.15), channel_id=1, source_target_pairs={{0,1},{1,2},{2,3},{3,0},{4,5},{5,6},{6,7},{7,4},{8,9},{9,10},{10,1... | collective-permute-start | bytes 1179656 | tf_op jit(solution)/shard_map/ppermute | solution.py:218
  9.5 3.6 %collective-permute-start.2 = (bf16[64,1024]{1,0:T(8,128)(2,1)}, bf16[64,1024]{1,0:T(8,128)(2,1)}, u32[]{:S(2)}, u32[]{:S(2)}) collective-permute-start(bf16[64,1024]{1,0:T(8,128)(2,1)} %get-tuple-element.16), channel_id=1, source_target_pairs={{0,2},{1,3},{2,0},{3,1},{4,6},{5,7},{6,4},{7,5},{8,10},{9,11},{10,... | collective-permute-start | bytes 393224 | tf_op jit(solution)/shard_map/ppermute | solution.py:217
  13.1 17.1 %all-to-all-start = ((bf16[64,8,128]{2,1,0:T(8,128)(2,1)}), bf16[64,8,128]{2,1,0:T(8,128)(2,1)S(1)}, u32[]{:S(2)}, u32[]{:S(2)}) async-start(bf16[64,8,128]{2,1,0:T(8,128)(2,1)} %bitcast.49), calls=%async_computation | async-start | bytes 262144 | tf_op jit(solution)/shard_map/all_to_all | solution.py:268
  30.2 0.0 copy-start.2
  30.2 0.0 copy-start
  30.2 0.0 copy-start.1
  30.3 0.6 copy-done.2
  30.9 0.0 copy-done
  30.9 0.0 copy-done.1
  30.9 0.3 shard_map.75
  31.2 0.0 collective-permute-done
  31.2 0.1 broadcast_in_dim.30
  31.3 4.1 %collective-permute-start.3 = (bf16[64,1024]{1,0:T(8,128)(2,1)S(1)}, bf16[64,1024]{1,0:T(8,128)(2,1)S(1)}, u32[]{:S(2)}, u32[]{:S(2)}) collective-permute-start(bf16[64,1024]{1,0:T(8,128)(2,1)S(1)} %get-tuple-element.22), channel_id=1, source_target_pairs={{0,3},{1,0},{2,1},{3,2},{4,7},{5,4},{6,5},{7,6},{8,11},{9,8},{10,9... | collective-permute-start | bytes 393224 | tf_op jit(solution)/shard_map/ppermute | solution.py:219
  35.4 0.0 collective-permute-done.1
  35.5 1.9 %collective-permute-start.4 = (bf16[64,1024]{1,0:T(8,128)(2,1)S(1)}, bf16[64,1024]{1,0:T(8,128)(2,1)S(1)}, u32[]{:S(2)}, u32[]{:S(2)}) collective-permute-start(bf16[64,1024]{1,0:T(8,128)(2,1)S(1)} %get-tuple-element.19), channel_id=1, source_target_pairs={{0,1},{1,2},{2,3},{3,0},{4,5},{5,6},{6,7},{7,4},{8,9},{9,10},{10,1... | collective-permute-start | bytes 393224 | tf_op jit(solution)/shard_map/ppermute | solution.py:220
  37.4 0.1 broadcast_in_dim.24
  37.6 0.0 copy-start.3
  37.6 1.0 copy-done.3
  38.6 6.6 %all-to-all-done = bf16[64,8,128]{2,1,0:T(8,128)(2,1)S(1)} async-done(((bf16[64,8,128]{2,1,0:T(8,128)(2,1)}), bf16[64,8,128]{2,1,0:T(8,128)(2,1)S(1)}, u32[]{:S(2)}, u32[]{:S(2)}) %all-to-all-start) | async-done | bytes 131104 | tf_op jit(solution)/shard_map/all_to_all | solution.py:268
  45.2 0.8 shard_map.74
  46.1 8.1 %all-to-all-start.1 = ((bf16[8,256,128]{2,1,0:T(8,128)(2,1)}), bf16[8,256,128]{2,1,0:T(8,128)(2,1)S(1)}, u32[]{:S(2)}, u32[]{:S(2)}) async-start(bf16[8,256,128]{2,1,0:T(8,128)(2,1)} %bitcast.10), calls=%async_computation.1 | async-start | bytes 1048576 | tf_op jit(solution)/shard_map/all_to_all | solution.py:279
  54.1 0.0 collective-permute-done.2
  54.1 0.9 bitcast_dynamic-update-slice_fusion.3
  55.0 0.0 collective-permute-done.3
  55.1 8.4 %all-to-all-done.1 = bf16[8,256,128]{2,1,0:T(8,128)(2,1)S(1)} async-done(((bf16[8,256,128]{2,1,0:T(8,128)(2,1)}), bf16[8,256,128]{2,1,0:T(8,128)(2,1)S(1)}, u32[]{:S(2)}, u32[]{:S(2)}) %all-to-all-start.1) | async-done | bytes 524320 | tf_op jit(solution)/shard_map/all_to_all | solution.py:279
  63.5 1.7 %shard_map.76 = bf16[4,256,256]{2,1,0:T(8,128)(2,1)} custom-call(bf16[2,16,64,128]{3,2,1,0:T(8,128)(2,1)S(1)} %bitcast.40, f32[1,1024]{1,0:T(1,128)S(1)} %get-tuple-element.14.gain_ref, bf16[4,2,64,1024]{3,2,1,0:T(8,128)(2,1)S(1)} %bitcast_dynamic-update-slice_fusion.2.weights_ref), custom_call_target="tpu_custom_call" | custom-call | flops 268435456 | bytes 1048576 | tf_op jit(solution)/shard_map/pallas_call | solution.py:195
  65.1 3.5 %all-to-all-start.2 = ((bf16[4,256,256]{2,1,0:T(8,128)(2,1)}), bf16[4,256,256]{2,1,0:T(8,128)(2,1)S(1)}, u32[]{:S(2)}, u32[]{:S(2)}) async-start(bf16[4,256,256]{2,1,0:T(8,128)(2,1)} %shard_map.76), calls=%async_computation.2 | async-start | bytes 1048576 | tf_op jit(solution)/shard_map/all_to_all | solution.py:298
  68.6 0.0 collective-permute-done.4
  68.7 9.2 %all-to-all-done.2.hidden_ref = bf16[4,256,256]{2,1,0:T(8,128)(2,1)S(1)} async-done(((bf16[4,256,256]{2,1,0:T(8,128)(2,1)}), bf16[4,256,256]{2,1,0:T(8,128)(2,1)S(1)}, u32[]{:S(2)}, u32[]{:S(2)}) %all-to-all-start.2) | async-done | bytes 524320 | tf_op jit(solution)/shard_map/all_to_all | solution.py:298
  77.9 0.4 shard_map.77
  78.3 26.8 %all_to_all.20 = bf16[128,4,128]{2,1,0:T(4,128)(2,1)S(1)} all-to-all(bf16[128,4,128]{2,1,0:T(4,128)(2,1)S(1)} %bitcast.42), channel_id=1, replica_groups=mesh['z'=16,'core'=2,'ty'=4,'tx'=4] {'z','core','tx'}, dimensions={0} | all-to-all | bytes 262144 | tf_op jit(solution)/shard_map/all_to_all | solution.py:308
  105.1 0.9 shard_map.78
  (8 shorter events, 0.2 us)
Async XLA Ops:
  2.3 28.9 %collective-permute-start = (bf16[3,64,1024]{2,1,0:T(8,128)(2,1)}, bf16[3,64,1024]{2,1,0:T(8,128)(2,1)S(1)}, u32[]{:S(2)}, u32[]{:S(2)}) collective-permute-start(bf16[3,64,1024]{2,1,0:T(8,128)(2,1)} %get-tuple-element.15), channel_id=1, source_target_pairs={{0,3},{1,0},{2,1},{3,2},{4,7},{5,4},{6,5},{7,6},{8,11},{9,8},{10,9... | collective-permute-start | bytes 1179656 | tf_op jit(solution)/shard_map/ppermute | solution.py:216
  7.5 27.9 %collective-permute-start.1 = (bf16[3,64,1024]{2,1,0:T(8,128)(2,1)}, bf16[3,64,1024]{2,1,0:T(8,128)(2,1)S(1)}, u32[]{:S(2)}, u32[]{:S(2)}) collective-permute-start(bf16[3,64,1024]{2,1,0:T(8,128)(2,1)} %get-tuple-element.15), channel_id=1, source_target_pairs={{0,1},{1,2},{2,3},{3,0},{4,5},{5,6},{6,7},{7,4},{8,9},{9,10},{10,1... | collective-permute-start | bytes 1179656 | tf_op jit(solution)/shard_map/ppermute | solution.py:218
  9.5 44.7 %collective-permute-start.2 = (bf16[64,1024]{1,0:T(8,128)(2,1)}, bf16[64,1024]{1,0:T(8,128)(2,1)}, u32[]{:S(2)}, u32[]{:S(2)}) collective-permute-start(bf16[64,1024]{1,0:T(8,128)(2,1)} %get-tuple-element.16), channel_id=1, source_target_pairs={{0,2},{1,3},{2,0},{3,1},{4,6},{5,7},{6,4},{7,5},{8,10},{9,11},{10,... | collective-permute-start | bytes 393224 | tf_op jit(solution)/shard_map/ppermute | solution.py:217
  13.1 32.1 %all-to-all-start = ((bf16[64,8,128]{2,1,0:T(8,128)(2,1)}), bf16[64,8,128]{2,1,0:T(8,128)(2,1)S(1)}, u32[]{:S(2)}, u32[]{:S(2)}) async-start(bf16[64,8,128]{2,1,0:T(8,128)(2,1)} %bitcast.49), calls=%async_computation | async-start | bytes 262144 | tf_op jit(solution)/shard_map/all_to_all | solution.py:268
  30.2 0.7 copy-start.2
  30.2 0.7 copy-start
  30.2 0.7 copy-start.1
  31.3 23.8 %collective-permute-start.3 = (bf16[64,1024]{1,0:T(8,128)(2,1)S(1)}, bf16[64,1024]{1,0:T(8,128)(2,1)S(1)}, u32[]{:S(2)}, u32[]{:S(2)}) collective-permute-start(bf16[64,1024]{1,0:T(8,128)(2,1)S(1)} %get-tuple-element.22), channel_id=1, source_target_pairs={{0,3},{1,0},{2,1},{3,2},{4,7},{5,4},{6,5},{7,6},{8,11},{9,8},{10,9... | collective-permute-start | bytes 393224 | tf_op jit(solution)/shard_map/ppermute | solution.py:219
  35.5 33.2 %collective-permute-start.4 = (bf16[64,1024]{1,0:T(8,128)(2,1)S(1)}, bf16[64,1024]{1,0:T(8,128)(2,1)S(1)}, u32[]{:S(2)}, u32[]{:S(2)}) collective-permute-start(bf16[64,1024]{1,0:T(8,128)(2,1)S(1)} %get-tuple-element.19), channel_id=1, source_target_pairs={{0,1},{1,2},{2,3},{3,0},{4,5},{5,6},{6,7},{7,4},{8,9},{9,10},{10,1... | collective-permute-start | bytes 393224 | tf_op jit(solution)/shard_map/ppermute | solution.py:220
  37.6 1.0 copy-start.3
  46.1 17.4 %all-to-all-start.1 = ((bf16[8,256,128]{2,1,0:T(8,128)(2,1)}), bf16[8,256,128]{2,1,0:T(8,128)(2,1)S(1)}, u32[]{:S(2)}, u32[]{:S(2)}) async-start(bf16[8,256,128]{2,1,0:T(8,128)(2,1)} %bitcast.10), calls=%async_computation.1 | async-start | bytes 1048576 | tf_op jit(solution)/shard_map/all_to_all | solution.py:279
  65.1 12.7 %all-to-all-start.2 = ((bf16[4,256,256]{2,1,0:T(8,128)(2,1)}), bf16[4,256,256]{2,1,0:T(8,128)(2,1)S(1)}, u32[]{:S(2)}, u32[]{:S(2)}) async-start(bf16[4,256,256]{2,1,0:T(8,128)(2,1)} %shard_map.76), calls=%async_computation.2 | async-start | bytes 1048576 | tf_op jit(solution)/shard_map/all_to_all | solution.py:298

commit v6 on v4

--- a/solution.py
+++ b/solution.py
@@ -59,7 +59,7 @@
     nz, cores, nx = sizes
     small = [(ids_hbm, ids_ref), (tokens_hbm, tokens_ref)]
     large = [(w, shard_ref.at[i]) for i, w in enumerate((gate_hbm, up_hbm, down_hbm))]
-    large += [(w, pair_ref.at[i]) for i, w in enumerate((gate_hbm, up_hbm))]
+    large += [(w, pair_ref.at[i]) for i, w in enumerate((gate_hbm, down_hbm))]
     copies = [pltpu.make_async_copy(a, b, sems.at[i]) for i, (a, b) in enumerate(small + large)]
     for copy in copies:
         copy.start()
@@ -214,18 +214,19 @@
         [(i, (i + hop) % count) for i in range(count)] for hop in (1, count - 2, count - 1)
     )
     right = lax.ppermute(shard, TX, after)
-    far_up = lax.ppermute(pair, TX, far)
+    across_pair = lax.ppermute(pair, TX, far)
     left = lax.ppermute(shard, TX, near)
-    far_down = lax.ppermute(right[2], TX, after)
+    far_up = lax.ppermute(right[1], TX, after)
     up = jnp.zeros((count, 2) + shard.shape[1:], shard.dtype)
     down = jnp.zeros((count,) + shard.shape[1:], shard.dtype)
     before, behind, across = (lax.rem(me + hop, count) for hop in (count - 1, 1, count - 2))
-    for piece, source in ((left, before), (right, behind), (shard, me)):
+    for piece, source in ((right, behind), (shard, me), (left, before)):
         up = set_at(up, piece[:2], source)
-    up = set_at(up, far_up, across)
+    for half, piece in enumerate((across_pair[0], far_up)):
+        up = lax.dynamic_update_slice(up, piece[None, None], (across, half, 0, 0))
     for piece, source in ((right, behind), (left, before), (shard, me)):
         down = set_at(down, piece[2], source)
-    down = set_at(down, far_down, across)
+    down = set_at(down, across_pair[1], across)
     return up, down
 
 

time: 104 us -> 104 us (level)
    unnamed x12 -> x8, local copies, waits for them, and re-layouts: 2.62 us -> 1.65 us
  transfers between devices with their start and end apart: 7 -> 7, of which waited for: 3 -> 3; matrix products, arithmetic and copies ran while one was open for 3% -> 4% of each run, Pallas kernels for 3% -> 1%
where the time goes in v6:
time: 104 us
  starting transfers between devices  43.5 us (42%)
  blocking collectives  24.3 us (23%)
  waiting for transfers between devices  23.4 us (22%)
  Pallas kernels  6.47 us (6%)
  local copies, waits for them, and re-layouts  5.65 us (5%)
    all_to_all x1, blocking collectives, body(): lax.all_to_all(out.reshape(ep * nx, inner, wide), (Z, CORE, TX), 0, 0, ti...  24.3 us
    all_to_all x1, starting transfers between devices, body(): lax.all_to_all(sent.reshape(nz * nx, cores * inner, wide), (Z, TX), 0, 0,...  17.1 us
    all_to_all x1, waiting for transfers between devices, body(): lax.all_to_all(spread.reshape(cores * ny, nx * nz * inner, wide), (CORE,...  8.38 us
    all_to_all x1, waiting for transfers between devices, body(): hidden = lax.all_to_all(hidden, TY, 0, 0, tiled=True)  8.3 us
    all_to_all x1, starting transfers between devices, body(): lax.all_to_all(spread.reshape(cores * ny, nx * nz * inner, wide), (CORE,...  8.06 us
    all_to_all x1, waiting for transfers between devices, body(): lax.all_to_all(sent.reshape(nz * nx, cores * inner, wide), (Z, TX), 0, 0,...  6.73 us
    pallas_call x6, Pallas kernels, call(): pl.pallas_call(kernel, out_shape=out_shapes, in_specs=[pl.BlockSpec(memor...  6.47 us
    ppermute x1, starting transfers between devices, gathered(): right = lax.ppermute(shard, TX, after)  5.2 us
  transfers between devices with their start and end apart: 7, of which 3 were waited for; matrix products, arithmetic and copies ran while one was open for 4% of the time, Pallas kernels for 1%

profile of v6, /device:TPU:1, one launch (start us, length us, event | category | flops | bytes accessed | tf_op | source)
XLA Modules:
  0.0 103.5 jit_solution(7086463795829286224)
XLA Ops:
  0.0 2.4 %shard_map.73 = (bf16[512,128]{1,0:T(8,128)(2,1)}, s32[4,128]{1,0:T(4,128)}, bf16[3,64,1024]{2,1,0:T(8,128)(2,1)}, bf16[2,64,1024]{2,1,0:T(8,128)(2,1)}) custom-call(s32[4,128]{1,0:T(4,128)} %bitcast.49, bf16[64,128]{1,0:T(8,128)(2,1)} %bitcast.48, bf16[64,1024]{1,0:T(8,128)(2,1)} %bitcast.44, bf16[64,1024]{1,0:T(8,128)(2,1)} %bitcast.45, ...), custom_call_target="tpu_custom_call" | custom-call | flops 16777216 | bytes 1048576 | tf_op jit(solution)/shard_map/pallas_call | solution.py:195
  2.4 5.2 %collective-permute-start = (bf16[3,64,1024]{2,1,0:T(8,128)(2,1)}, bf16[3,64,1024]{2,1,0:T(8,128)(2,1)S(1)}, u32[]{:S(2)}, u32[]{:S(2)}) collective-permute-start(bf16[3,64,1024]{2,1,0:T(8,128)(2,1)} %get-tuple-element.15), channel_id=1, source_target_pairs={{0,3},{1,0},{2,1},{3,2},{4,7},{5,4},{6,5},{7,6},{8,11},{9,8},{10,9... | collective-permute-start | bytes 1179656 | tf_op jit(solution)/shard_map/ppermute | solution.py:216
  7.6 1.9 %collective-permute-start.1 = (bf16[3,64,1024]{2,1,0:T(8,128)(2,1)}, bf16[3,64,1024]{2,1,0:T(8,128)(2,1)}, u32[]{:S(2)}, u32[]{:S(2)}) collective-permute-start(bf16[3,64,1024]{2,1,0:T(8,128)(2,1)} %get-tuple-element.15), channel_id=1, source_target_pairs={{0,1},{1,2},{2,3},{3,0},{4,5},{5,6},{6,7},{7,4},{8,9},{9,10},{10,1... | collective-permute-start | bytes 1179656 | tf_op jit(solution)/shard_map/ppermute | solution.py:218
  9.6 3.6 %collective-permute-start.2 = (bf16[2,64,1024]{2,1,0:T(8,128)(2,1)}, bf16[2,64,1024]{2,1,0:T(8,128)(2,1)}, u32[]{:S(2)}, u32[]{:S(2)}) collective-permute-start(bf16[2,64,1024]{2,1,0:T(8,128)(2,1)} %get-tuple-element.16), channel_id=1, source_target_pairs={{0,2},{1,3},{2,0},{3,1},{4,6},{5,7},{6,4},{7,5},{8,10},{9,11},{10,... | collective-permute-start | bytes 786440 | tf_op jit(solution)/shard_map/ppermute | solution.py:217
  13.2 17.1 %all-to-all-start = ((bf16[64,8,128]{2,1,0:T(8,128)(2,1)}), bf16[64,8,128]{2,1,0:T(8,128)(2,1)S(1)}, u32[]{:S(2)}, u32[]{:S(2)}) async-start(bf16[64,8,128]{2,1,0:T(8,128)(2,1)} %bitcast.47), calls=%async_computation | async-start | bytes 262144 | tf_op jit(solution)/shard_map/all_to_all | solution.py:267
  30.3 0.0 copy-start.2
  30.3 0.0 copy-start
  30.3 0.0 copy-start.1
  30.3 0.6 copy-done.2
  31.0 0.0 copy-done
  31.0 0.0 copy-done.1
  31.0 0.3 shard_map.75
  31.3 0.0 collective-permute-done
  31.3 0.1 broadcast_in_dim.23
  31.4 4.1 %collective-permute-start.3 = (bf16[64,1024]{1,0:T(8,128)(2,1)S(1)}, bf16[64,1024]{1,0:T(8,128)(2,1)S(1)}, u32[]{:S(2)}, u32[]{:S(2)}) collective-permute-start(bf16[64,1024]{1,0:T(8,128)(2,1)S(1)} %get-tuple-element.20), channel_id=1, source_target_pairs={{0,3},{1,0},{2,1},{3,2},{4,7},{5,4},{6,5},{7,6},{8,11},{9,8},{10,9... | collective-permute-start | bytes 393224 | tf_op jit(solution)/shard_map/ppermute | solution.py:219
  35.5 0.1 broadcast_in_dim.18
  35.6 0.0 copy-start.3
  35.7 1.0 copy-done.3
  36.7 0.0 collective-permute-done.1
  36.7 0.9 slice_dynamic-update-slice_fusion.1
  37.6 1.0 fusion
  38.6 6.7 %all-to-all-done = bf16[64,8,128]{2,1,0:T(8,128)(2,1)S(1)} async-done(((bf16[64,8,128]{2,1,0:T(8,128)(2,1)}), bf16[64,8,128]{2,1,0:T(8,128)(2,1)S(1)}, u32[]{:S(2)}, u32[]{:S(2)}) %all-to-all-start) | async-done | bytes 131104 | tf_op jit(solution)/shard_map/all_to_all | solution.py:267
  45.3 0.8 shard_map.74
  46.2 8.1 %all-to-all-start.1 = ((bf16[8,256,128]{2,1,0:T(8,128)(2,1)}), bf16[8,256,128]{2,1,0:T(8,128)(2,1)S(1)}, u32[]{:S(2)}, u32[]{:S(2)}) async-start(bf16[8,256,128]{2,1,0:T(8,128)(2,1)} %bitcast.10), calls=%async_computation.1 | async-start | bytes 1048576 | tf_op jit(solution)/shard_map/all_to_all | solution.py:278
  54.2 0.0 collective-permute-done.2
  54.2 0.9 fusion.2
  55.1 0.0 collective-permute-done.3
  55.2 8.4 %all-to-all-done.1 = bf16[8,256,128]{2,1,0:T(8,128)(2,1)S(1)} async-done(((bf16[8,256,128]{2,1,0:T(8,128)(2,1)}), bf16[8,256,128]{2,1,0:T(8,128)(2,1)S(1)}, u32[]{:S(2)}, u32[]{:S(2)}) %all-to-all-start.1) | async-done | bytes 524320 | tf_op jit(solution)/shard_map/all_to_all | solution.py:278
  63.5 1.7 %shard_map.76 = bf16[4,256,256]{2,1,0:T(8,128)(2,1)} custom-call(bf16[2,16,64,128]{3,2,1,0:T(8,128)(2,1)S(1)} %bitcast.38, f32[1,1024]{1,0:T(1,128)S(1)} %get-tuple-element.14.gain_ref, bf16[4,2,64,1024]{3,2,1,0:T(8,128)(2,1)S(1)} %bitcast_dynamic-update-slice_fusion.1.weights_ref), custom_call_target="tpu_custom_call" | custom-call | flops 268435456 | bytes 1048576 | tf_op jit(solution)/shard_map/pallas_call | solution.py:195
  65.2 3.5 %all-to-all-start.2 = ((bf16[4,256,256]{2,1,0:T(8,128)(2,1)}), bf16[4,256,256]{2,1,0:T(8,128)(2,1)S(1)}, u32[]{:S(2)}, u32[]{:S(2)}) async-start(bf16[4,256,256]{2,1,0:T(8,128)(2,1)} %shard_map.76), calls=%async_computation.2 | async-start | bytes 1048576 | tf_op jit(solution)/shard_map/all_to_all | solution.py:297
  68.7 0.9 slice_dynamic-update-slice_fusion.weights_ref
  69.6 8.3 %all-to-all-done.2.hidden_ref = bf16[4,256,256]{2,1,0:T(8,128)(2,1)S(1)} async-done(((bf16[4,256,256]{2,1,0:T(8,128)(2,1)}), bf16[4,256,256]{2,1,0:T(8,128)(2,1)S(1)}, u32[]{:S(2)}, u32[]{:S(2)}) %all-to-all-start.2) | async-done | bytes 524320 | tf_op jit(solution)/shard_map/all_to_all | solution.py:297
  77.9 0.4 shard_map.77
  78.3 24.3 %all_to_all.20 = bf16[128,4,128]{2,1,0:T(4,128)(2,1)S(1)} all-to-all(bf16[128,4,128]{2,1,0:T(4,128)(2,1)S(1)} %bitcast.40), channel_id=1, replica_groups=mesh['z'=16,'core'=2,'ty'=4,'tx'=4] {'z','core','tx'}, dimensions={0} | all-to-all | bytes 262144 | tf_op jit(solution)/shard_map/all_to_all | solution.py:307
  102.7 0.9 shard_map.78
  (5 shorter events, 0.1 us)
Async XLA Ops:
  2.4 28.9 %collective-permute-start = (bf16[3,64,1024]{2,1,0:T(8,128)(2,1)}, bf16[3,64,1024]{2,1,0:T(8,128)(2,1)S(1)}, u32[]{:S(2)}, u32[]{:S(2)}) collective-permute-start(bf16[3,64,1024]{2,1,0:T(8,128)(2,1)} %get-tuple-element.15), channel_id=1, source_target_pairs={{0,3},{1,0},{2,1},{3,2},{4,7},{5,4},{6,5},{7,6},{8,11},{9,8},{10,9... | collective-permute-start | bytes 1179656 | tf_op jit(solution)/shard_map/ppermute | solution.py:216
  7.6 29.0 %collective-permute-start.1 = (bf16[3,64,1024]{2,1,0:T(8,128)(2,1)}, bf16[3,64,1024]{2,1,0:T(8,128)(2,1)}, u32[]{:S(2)}, u32[]{:S(2)}) collective-permute-start(bf16[3,64,1024]{2,1,0:T(8,128)(2,1)} %get-tuple-element.15), channel_id=1, source_target_pairs={{0,1},{1,2},{2,3},{3,0},{4,5},{5,6},{6,7},{7,4},{8,9},{9,10},{10,1... | collective-permute-start | bytes 1179656 | tf_op jit(solution)/shard_map/ppermute | solution.py:218
  9.6 44.6 %collective-permute-start.2 = (bf16[2,64,1024]{2,1,0:T(8,128)(2,1)}, bf16[2,64,1024]{2,1,0:T(8,128)(2,1)}, u32[]{:S(2)}, u32[]{:S(2)}) collective-permute-start(bf16[2,64,1024]{2,1,0:T(8,128)(2,1)} %get-tuple-element.16), channel_id=1, source_target_pairs={{0,2},{1,3},{2,0},{3,1},{4,6},{5,7},{6,4},{7,5},{8,10},{9,11},{10,... | collective-permute-start | bytes 786440 | tf_op jit(solution)/shard_map/ppermute | solution.py:217
  13.2 32.1 %all-to-all-start = ((bf16[64,8,128]{2,1,0:T(8,128)(2,1)}), bf16[64,8,128]{2,1,0:T(8,128)(2,1)S(1)}, u32[]{:S(2)}, u32[]{:S(2)}) async-start(bf16[64,8,128]{2,1,0:T(8,128)(2,1)} %bitcast.47), calls=%async_computation | async-start | bytes 262144 | tf_op jit(solution)/shard_map/all_to_all | solution.py:267
  30.3 0.7 copy-start.2
  30.3 0.7 copy-start
  30.3 0.7 copy-start.1
  31.4 23.7 %collective-permute-start.3 = (bf16[64,1024]{1,0:T(8,128)(2,1)S(1)}, bf16[64,1024]{1,0:T(8,128)(2,1)S(1)}, u32[]{:S(2)}, u32[]{:S(2)}) collective-permute-start(bf16[64,1024]{1,0:T(8,128)(2,1)S(1)} %get-tuple-element.20), channel_id=1, source_target_pairs={{0,3},{1,0},{2,1},{3,2},{4,7},{5,4},{6,5},{7,6},{8,11},{9,8},{10,9... | collective-permute-start | bytes 393224 | tf_op jit(solution)/shard_map/ppermute | solution.py:219
  35.6 1.0 copy-start.3
  46.2 17.4 %all-to-all-start.1 = ((bf16[8,256,128]{2,1,0:T(8,128)(2,1)}), bf16[8,256,128]{2,1,0:T(8,128)(2,1)S(1)}, u32[]{:S(2)}, u32[]{:S(2)}) async-start(bf16[8,256,128]{2,1,0:T(8,128)(2,1)} %bitcast.10), calls=%async_computation.1 | async-start | bytes 1048576 | tf_op jit(solution)/shard_map/all_to_all | solution.py:278
  65.2 12.7 %all-to-all-start.2 = ((bf16[4,256,256]{2,1,0:T(8,128)(2,1)}), bf16[4,256,256]{2,1,0:T(8,128)(2,1)S(1)}, u32[]{:S(2)}, u32[]{:S(2)}) async-start(bf16[4,256,256]{2,1,0:T(8,128)(2,1)} %shard_map.76), calls=%async_computation.2 | async-start | bytes 1048576 | tf_op jit(solution)/shard_map/all_to_all | solution.py:297

commit v7 on v3

--- a/solution.py
+++ b/solution.py
@@ -125,7 +125,7 @@
                 out_ref[core, c, x] = part
 
 
-def up_kernel(rows_ref, gain_ref, weights_ref, out_ref, whole, normed):
+def norm_kernel(rows_ref, gain_ref, normed, whole):
     cores, pieces, part, wide = rows_ref.shape
     group = cores * part
     full = normed.shape[1]
@@ -144,7 +144,10 @@
         inverse = lax.rsqrt(mean + EPSILON)
         rows = slice(h * group, (h + 1) * group)
         normed[rows] = (whole[rows] * inverse * gain_ref[...]).astype(BF16)
-    nx, _, units, _ = weights_ref.shape
+
+
+def up_kernel(normed, weights_ref, out_ref):
+    nx, _, units, full = weights_ref.shape
     w_gate = weights_ref[:, 0].reshape(nx * units, full)
     w_up = weights_ref[:, 1].reshape(nx * units, full)
     gate = jnp.minimum(dot_nt(normed[...], w_gate), LIMIT)
@@ -280,15 +283,14 @@
         route_weight.astype(F32).T,
         norm_gain.astype(F32).reshape(1, full),
     )
-    hidden = call(
-        up_kernel,
-        shape((ny, 2 * group, nx * units), BF16),
+    normed = call(
+        norm_kernel,
+        shape((2 * group, full), BF16),
         rows.reshape(cores, tp, nz * inner, wide),
         gain,
-        w_up,
-        flops=1 << 28,
-        scratch=(pltpu.VMEM((2 * group, full), F32), pltpu.VMEM((2 * group, full), BF16)),
-    )
+        scratch=(pltpu.VMEM((2 * group, full), F32),),
+    )
+    hidden = call(up_kernel, shape((ny, 2 * group, nx * units), BF16), normed, w_up, flops=1 << 28)
     hidden = lax.all_to_all(hidden, TY, 0, 0, tiled=True)
     out = call(
         functools.partial(down_kernel, cores),

time: 103 us -> 102 us (level)
    pallas_call x6 -> x7, Pallas kernels: 6.33 us -> 6.37 us  [call(): pl.pallas_call(kernel, out_shape=out_shapes, in_specs=[pl.BlockSpec(memor...]
where the time goes in v7:
time: 102 us; the launch traced here: 101 us
  starting transfers between devices  42.3 us (41%)
  blocking collectives  25.4 us (25%)
  waiting for transfers between devices  24.2 us (24%)
  Pallas kernels  6.37 us (6%)
  local copies, waits for them, and re-layouts  2.7 us (3%)
    all_to_all x1, blocking collectives, body(): lax.all_to_all(out.reshape(ep * nx, inner, wide), (Z, CORE, TX), 0, 0, ti...  25.4 us
    all_to_all x1, starting transfers between devices, body(): lax.all_to_all(sent.reshape(nz * nx, cores * inner, wide), (Z, TX), 0, 0,...  17.3 us
    all_to_all x1, waiting for transfers between devices, body(): hidden = lax.all_to_all(hidden, TY, 0, 0, tiled=True)  9.19 us
    all_to_all x1, waiting for transfers between devices, body(): lax.all_to_all(spread.reshape(cores * ny, nx * nz * inner, wide), (CORE,...  8.32 us
    all_to_all x1, starting transfers between devices, body(): lax.all_to_all(spread.reshape(cores * ny, nx * nz * inner, wide), (CORE,...  7.91 us
    all_to_all x1, waiting for transfers between devices, body(): lax.all_to_all(sent.reshape(nz * nx, cores * inner, wide), (Z, TX), 0, 0,...  6.65 us
    pallas_call x7, Pallas kernels, call(): pl.pallas_call(kernel, out_shape=out_shapes, in_specs=[pl.BlockSpec(memor...  6.37 us
    ppermute x1, starting transfers between devices, gathered(): left = lax.ppermute(shard, TX, near)  3.94 us
  transfers between devices with their start and end apart: 7, of which 3 were waited for; matrix products, arithmetic and copies ran while one was open for 2% of the time, Pallas kernels for 3%

profile of v7, /device:TPU:1, one launch (start us, length us, event | category | flops | bytes accessed | tf_op | source)
XLA Modules:
  0.0 101.1 jit_solution(666940200765433998)
XLA Ops:
  0.0 2.3 %shard_map.73 = (bf16[512,128]{1,0:T(8,128)(2,1)}, s32[4,128]{1,0:T(4,128)}, bf16[3,64,1024]{2,1,0:T(8,128)(2,1)}) custom-call(s32[4,128]{1,0:T(4,128)} %bitcast.45, bf16[64,128]{1,0:T(8,128)(2,1)} %bitcast.44, bf16[64,1024]{1,0:T(8,128)(2,1)} %bitcast.40, bf16[64,1024]{1,0:T(8,128)(2,1)} %bitcast.41, bf16[64,1024]{1,0:T(8,128)(2,1)} %bitcast.42), custom_call_target="tpu_custom_call" | custom-call | flops 16777216 | bytes 1048576 | tf_op jit(solution)/shard_map/pallas_call | solution.py:197
  2.3 3.9 %collective-permute-start = (bf16[3,64,1024]{2,1,0:T(8,128)(2,1)}, bf16[3,64,1024]{2,1,0:T(8,128)(2,1)S(1)}, u32[]{:S(2)}, u32[]{:S(2)}) collective-permute-start(bf16[3,64,1024]{2,1,0:T(8,128)(2,1)} %get-tuple-element.14), channel_id=1, source_target_pairs={{0,1},{1,2},{2,3},{3,0},{4,5},{5,6},{6,7},{7,4},{8,9},{9,10},{10,1... | collective-permute-start | bytes 1179656 | tf_op jit(solution)/shard_map/ppermute | solution.py:216
  6.2 3.2 %collective-permute-start.1 = (bf16[3,64,1024]{2,1,0:T(8,128)(2,1)}, bf16[3,64,1024]{2,1,0:T(8,128)(2,1)S(1)}, u32[]{:S(2)}, u32[]{:S(2)}) collective-permute-start(bf16[3,64,1024]{2,1,0:T(8,128)(2,1)} %get-tuple-element.14), channel_id=1, source_target_pairs={{0,3},{1,0},{2,1},{3,2},{4,7},{5,4},{6,5},{7,6},{8,11},{9,8},{10,9... | collective-permute-start | bytes 1179656 | tf_op jit(solution)/shard_map/ppermute | solution.py:217
  9.4 17.3 %all-to-all-start = ((bf16[64,8,128]{2,1,0:T(8,128)(2,1)}), bf16[64,8,128]{2,1,0:T(8,128)(2,1)S(1)}, u32[]{:S(2)}, u32[]{:S(2)}) async-start(bf16[64,8,128]{2,1,0:T(8,128)(2,1)} %bitcast.43), calls=%async_computation | async-start | bytes 262144 | tf_op jit(solution)/shard_map/all_to_all | solution.py:265
  26.7 0.0 copy-start.2
  26.7 0.0 copy-start
  26.8 0.0 copy-start.1
  26.8 0.6 copy-done.2
  27.4 0.0 copy-done
  27.4 0.0 copy-done.1
  27.4 0.3 shard_map.75
  27.7 0.0 collective-permute-done
  27.7 0.7 slice.26
  28.4 2.9 %collective-permute-start.2 = (bf16[2,64,1024]{2,1,0:T(8,128)(2,1)}, bf16[2,64,1024]{2,1,0:T(8,128)(2,1)}, u32[]{:S(2)}, u32[]{:S(2)}) collective-permute-start(bf16[2,64,1024]{2,1,0:T(8,128)(2,1)} %slice.26), channel_id=1, source_target_pairs={{0,1},{1,2},{2,3},{3,0},{4,5},{5,6},{6,7},{7,4},{8,9},{9,10},{10,1... | collective-permute-start | bytes 786440 | tf_op jit(solution)/shard_map/ppermute | solution.py:218
  31.4 0.1 broadcast_in_dim.26
  31.4 0.0 collective-permute-done.1
  31.5 3.6 %collective-permute-start.3 = (bf16[64,1024]{1,0:T(8,128)(2,1)S(1)}, bf16[64,1024]{1,0:T(8,128)(2,1)S(1)}, u32[]{:S(2)}, u32[]{:S(2)}) collective-permute-start(bf16[64,1024]{1,0:T(8,128)(2,1)S(1)} %get-tuple-element.17), channel_id=1, source_target_pairs={{0,3},{1,0},{2,1},{3,2},{4,7},{5,4},{6,5},{7,6},{8,11},{9,8},{10,9... | collective-permute-start | bytes 393224 | tf_op jit(solution)/shard_map/ppermute | solution.py:219
  35.1 0.1 broadcast_in_dim.21
  35.3 6.7 %all-to-all-done = bf16[64,8,128]{2,1,0:T(8,128)(2,1)S(1)} async-done(((bf16[64,8,128]{2,1,0:T(8,128)(2,1)}), bf16[64,8,128]{2,1,0:T(8,128)(2,1)S(1)}, u32[]{:S(2)}, u32[]{:S(2)}) %all-to-all-start) | async-done | bytes 131104 | tf_op jit(solution)/shard_map/all_to_all | solution.py:265
  41.9 0.8 shard_map.74
  42.7 0.0 copy-start.3
  42.7 7.9 %all-to-all-start.1 = ((bf16[8,256,128]{2,1,0:T(8,128)(2,1)}), bf16[8,256,128]{2,1,0:T(8,128)(2,1)S(1)}, u32[]{:S(2)}, u32[]{:S(2)}) async-start(bf16[8,256,128]{2,1,0:T(8,128)(2,1)} %bitcast.10), calls=%async_computation.1 | async-start | bytes 1048576 | tf_op jit(solution)/shard_map/all_to_all | solution.py:276
  50.7 0.0 copy-done.3
  50.7 0.0 collective-permute-done.2
  50.7 1.0 bitcast_dynamic-update-slice_fusion.weights_ref
  51.7 8.3 %all-to-all-done.1 = bf16[8,256,128]{2,1,0:T(8,128)(2,1)S(1)} async-done(((bf16[8,256,128]{2,1,0:T(8,128)(2,1)}), bf16[8,256,128]{2,1,0:T(8,128)(2,1)S(1)}, u32[]{:S(2)}, u32[]{:S(2)}) %all-to-all-start.1) | async-done | bytes 524320 | tf_op jit(solution)/shard_map/all_to_all | solution.py:276
  60.0 0.4 shard_map.76.normed
  60.4 1.3 %shard_map.77 = bf16[4,256,256]{2,1,0:T(8,128)(2,1)} custom-call(bf16[256,1024]{1,0:T(8,128)(2,1)S(1)} %shard_map.76.normed, bf16[4,2,64,1024]{3,2,1,0:T(8,128)(2,1)S(1)} %bitcast_dynamic-update-slice_fusion.weights_ref), custom_call_target="tpu_custom_call" | custom-call | flops 268435456 | bytes 1048576 | tf_op jit(solution)/shard_map/pallas_call | solution.py:197
  61.7 3.5 %all-to-all-start.2 = ((bf16[4,256,256]{2,1,0:T(8,128)(2,1)}), bf16[4,256,256]{2,1,0:T(8,128)(2,1)S(1)}, u32[]{:S(2)}, u32[]{:S(2)}) async-start(bf16[4,256,256]{2,1,0:T(8,128)(2,1)} %shard_map.77), calls=%async_computation.2 | async-start | bytes 1048576 | tf_op jit(solution)/shard_map/all_to_all | solution.py:294
  65.2 0.0 collective-permute-done.3
  65.2 9.2 %all-to-all-done.2.hidden_ref = bf16[4,256,256]{2,1,0:T(8,128)(2,1)S(1)} async-done(((bf16[4,256,256]{2,1,0:T(8,128)(2,1)}), bf16[4,256,256]{2,1,0:T(8,128)(2,1)S(1)}, u32[]{:S(2)}, u32[]{:S(2)}) %all-to-all-start.2) | async-done | bytes 524320 | tf_op jit(solution)/shard_map/all_to_all | solution.py:294
  74.4 0.4 shard_map.78
  74.8 25.4 %all_to_all.20 = bf16[128,4,128]{2,1,0:T(4,128)(2,1)S(1)} all-to-all(bf16[128,4,128]{2,1,0:T(4,128)(2,1)S(1)} %bitcast.36), channel_id=1, replica_groups=mesh['z'=16,'core'=2,'ty'=4,'tx'=4] {'z','core','tx'}, dimensions={0} | all-to-all | bytes 262144 | tf_op jit(solution)/shard_map/all_to_all | solution.py:304
  100.2 0.9 shard_map.79
  (7 shorter events, 0.1 us)
Async XLA Ops:
  2.3 25.4 %collective-permute-start = (bf16[3,64,1024]{2,1,0:T(8,128)(2,1)}, bf16[3,64,1024]{2,1,0:T(8,128)(2,1)S(1)}, u32[]{:S(2)}, u32[]{:S(2)}) collective-permute-start(bf16[3,64,1024]{2,1,0:T(8,128)(2,1)} %get-tuple-element.14), channel_id=1, source_target_pairs={{0,1},{1,2},{2,3},{3,0},{4,5},{5,6},{6,7},{7,4},{8,9},{9,10},{10,1... | collective-permute-start | bytes 1179656 | tf_op jit(solution)/shard_map/ppermute | solution.py:216
  6.2 25.2 %collective-permute-start.1 = (bf16[3,64,1024]{2,1,0:T(8,128)(2,1)}, bf16[3,64,1024]{2,1,0:T(8,128)(2,1)S(1)}, u32[]{:S(2)}, u32[]{:S(2)}) collective-permute-start(bf16[3,64,1024]{2,1,0:T(8,128)(2,1)} %get-tuple-element.14), channel_id=1, source_target_pairs={{0,3},{1,0},{2,1},{3,2},{4,7},{5,4},{6,5},{7,6},{8,11},{9,8},{10,9... | collective-permute-start | bytes 1179656 | tf_op jit(solution)/shard_map/ppermute | solution.py:217
  9.4 32.5 %all-to-all-start = ((bf16[64,8,128]{2,1,0:T(8,128)(2,1)}), bf16[64,8,128]{2,1,0:T(8,128)(2,1)S(1)}, u32[]{:S(2)}, u32[]{:S(2)}) async-start(bf16[64,8,128]{2,1,0:T(8,128)(2,1)} %bitcast.43), calls=%async_computation | async-start | bytes 262144 | tf_op jit(solution)/shard_map/all_to_all | solution.py:265
  26.7 0.7 copy-start.2
  26.7 0.7 copy-start
  26.8 0.7 copy-start.1
  28.4 22.2 %collective-permute-start.2 = (bf16[2,64,1024]{2,1,0:T(8,128)(2,1)}, bf16[2,64,1024]{2,1,0:T(8,128)(2,1)}, u32[]{:S(2)}, u32[]{:S(2)}) collective-permute-start(bf16[2,64,1024]{2,1,0:T(8,128)(2,1)} %slice.26), channel_id=1, source_target_pairs={{0,1},{1,2},{2,3},{3,0},{4,5},{5,6},{6,7},{7,4},{8,9},{9,10},{10,1... | collective-permute-start | bytes 786440 | tf_op jit(solution)/shard_map/ppermute | solution.py:218
  31.5 33.7 %collective-permute-start.3 = (bf16[64,1024]{1,0:T(8,128)(2,1)S(1)}, bf16[64,1024]{1,0:T(8,128)(2,1)S(1)}, u32[]{:S(2)}, u32[]{:S(2)}) collective-permute-start(bf16[64,1024]{1,0:T(8,128)(2,1)S(1)} %get-tuple-element.17), channel_id=1, source_target_pairs={{0,3},{1,0},{2,1},{3,2},{4,7},{5,4},{6,5},{7,6},{8,11},{9,8},{10,9... | collective-permute-start | bytes 393224 | tf_op jit(solution)/shard_map/ppermute | solution.py:219
  42.7 7.9 %copy-start.3 = (bf16[3,64,1024]{2,1,0:T(8,128)(2,1)S(1)}, bf16[3,64,1024]{2,1,0:T(8,128)(2,1)}, u32[]{:S(2)}) copy-start(bf16[3,64,1024]{2,1,0:T(8,128)(2,1)} %get-tuple-element.14) | copy-start | bytes 1179652
  42.7 17.2 %all-to-all-start.1 = ((bf16[8,256,128]{2,1,0:T(8,128)(2,1)}), bf16[8,256,128]{2,1,0:T(8,128)(2,1)S(1)}, u32[]{:S(2)}, u32[]{:S(2)}) async-start(bf16[8,256,128]{2,1,0:T(8,128)(2,1)} %bitcast.10), calls=%async_computation.1 | async-start | bytes 1048576 | tf_op jit(solution)/shard_map/all_to_all | solution.py:276
  61.7 12.7 %all-to-all-start.2 = ((bf16[4,256,256]{2,1,0:T(8,128)(2,1)}), bf16[4,256,256]{2,1,0:T(8,128)(2,1)S(1)}, u32[]{:S(2)}, u32[]{:S(2)}) async-start(bf16[4,256,256]{2,1,0:T(8,128)(2,1)} %shard_map.77), calls=%async_computation.2 | async-start | bytes 1048576 | tf_op jit(solution)/shard_map/all_to_all | solution.py:294

commit v8 on v7

--- a/solution.py
+++ b/solution.py
@@ -212,18 +212,28 @@
 def gathered(shard):
     count = lax.axis_size(TX)
     me = lax.axis_index(TX)
-    near, after = ([(i, (i + hop) % count) for i in range(count)] for hop in (1, count - 1))
-    left = lax.ppermute(shard, TX, near)
-    right = lax.ppermute(shard, TX, after)
-    far_up = lax.ppermute(left[:2], TX, near)
-    far_down = lax.ppermute(right[2], TX, after)
+    core = lax.axis_index(CORE)
+
+    def hops(step):
+        return [
+            (c * count + i, c * count + (i + (step if c == 0 else -step)) % count)
+            for c in range(lax.axis_size(CORE))
+            for i in range(count)
+        ]
+
+    near, after, ring = hops(1), hops(-1), (CORE, TX)
+    left = lax.ppermute(shard, ring, near)
+    right = lax.ppermute(shard, ring, after)
+    far_up = lax.ppermute(left[:2], ring, near)
+    far_down = lax.ppermute(right[2], ring, after)
     up = jnp.zeros((count, 2) + shard.shape[1:], shard.dtype)
     down = jnp.zeros((count,) + shard.shape[1:], shard.dtype)
-    before, behind, across = (lax.rem(me + hop, count) for hop in (count - 1, 1, count - 2))
+    one = jnp.where(core == 0, 1, count - 1)
+    before, behind, across = (lax.rem(me + hop, count) for hop in (count - one, one, count - 2))
     for piece, source in ((left, before), (right, behind), (shard, me)):
         up = set_at(up, piece[:2], source)
     up = set_at(up, far_up, across)
-    for piece, source in ((left, before), (right, behind), (shard, me)):
+    for piece, source in ((left, before), (shard, me), (right, behind)):
         down = set_at(down, piece[2], source)
     down = set_at(down, far_down, across)
     return up, down

time: 102 us -> 101 us (level)
  local copies, waits for them, and re-layouts: 2.7 us -> 4.55 us
  waiting for transfers between devices: 24.2 us -> 22.6 us
  blocking collectives: 25.4 us -> 24.1 us
    all_to_all x1, waiting for transfers between devices: 9.19 us -> 1.98 us  [body(): hidden = lax.all_to_all(hidden, TY, 0, 0, tiled=True)]
    ppermute x4, waiting for transfers between devices: 0.01 us -> 5.04 us  [the longest x1 5.04 us: gathered(): far_down = lax.ppermute(right[2], ring, after)]
    all_to_all x1, waiting for transfers between devices: 6.65 us -> 8.18 us  [body(): lax.all_to_all(sent.reshape(nz * nx, cores * inner, wide), (Z, TX), 0, 0,...]
    all_to_all x1, blocking collectives: 25.4 us -> 24.1 us  [body(): lax.all_to_all(out.reshape(ep * nx, inner, wide), (Z, CORE, TX), 0, 0, ti...]
  transfers between devices with their start and end apart: 7 -> 7, of which waited for: 3 -> 4; matrix products, arithmetic and copies ran while one was open for 2% -> 3% of each run, Pallas kernels for 3% -> 1%
where the time goes in v8:
time: 101 us
  starting transfers between devices  42.8 us (42%)
  blocking collectives  24.1 us (24%)
  waiting for transfers between devices  22.6 us (22%)
  Pallas kernels  6.36 us (6%)
  local copies, waits for them, and re-layouts  4.55 us (5%)
    all_to_all x1, blocking collectives, body(): lax.all_to_all(out.reshape(ep * nx, inner, wide), (Z, CORE, TX), 0, 0, ti...  24.1 us
    all_to_all x1, starting transfers between devices, body(): lax.all_to_all(sent.reshape(nz * nx, cores * inner, wide), (Z, TX), 0, 0,...  18.2 us
    all_to_all x1, waiting for transfers between devices, body(): lax.all_to_all(sent.reshape(nz * nx, cores * inner, wide), (Z, TX), 0, 0,...  8.18 us
    all_to_all x1, starting transfers between devices, body(): lax.all_to_all(spread.reshape(cores * ny, nx * nz * inner, wide), (CORE,...  7.75 us
    all_to_all x1, waiting for transfers between devices, body(): lax.all_to_all(spread.reshape(cores * ny, nx * nz * inner, wide), (CORE,...  7.43 us
    pallas_call x7, Pallas kernels, call(): pl.pallas_call(kernel, out_shape=out_shapes, in_specs=[pl.BlockSpec(memor...  6.36 us
    ppermute x1, starting transfers between devices, gathered(): left = lax.ppermute(shard, ring, near)  5.2 us
    ppermute x1, waiting for transfers between devices, gathered(): far_down = lax.ppermute(right[2], ring, after)  5.04 us
  transfers between devices with their start and end apart: 7, of which 4 were waited for; matrix products, arithmetic and copies ran while one was open for 3% of the time, Pallas kernels for 1%

profile of v8, /device:TPU:1, one launch (start us, length us, event | category | flops | bytes accessed | tf_op | source)
XLA Modules:
  0.0 100.7 jit_solution(15055197435061285725)
XLA Ops:
  0.0 2.3 %shard_map.73 = (bf16[512,128]{1,0:T(8,128)(2,1)}, s32[4,128]{1,0:T(4,128)}, bf16[3,64,1024]{2,1,0:T(8,128)(2,1)}) custom-call(s32[4,128]{1,0:T(4,128)} %bitcast.45, bf16[64,128]{1,0:T(8,128)(2,1)} %bitcast.44, bf16[64,1024]{1,0:T(8,128)(2,1)} %bitcast.40, bf16[64,1024]{1,0:T(8,128)(2,1)} %bitcast.41, bf16[64,1024]{1,0:T(8,128)(2,1)} %bitcast.42), custom_call_target="tpu_custom_call" | custom-call | flops 16777216 | bytes 1048576 | tf_op jit(solution)/shard_map/pallas_call | solution.py:197
  2.3 5.2 %collective-permute-start = (bf16[3,64,1024]{2,1,0:T(8,128)(2,1)}, bf16[3,64,1024]{2,1,0:T(8,128)(2,1)S(1)}, u32[]{:S(2)}, u32[]{:S(2)}) collective-permute-start(bf16[3,64,1024]{2,1,0:T(8,128)(2,1)} %get-tuple-element.14), channel_id=1, source_target_pairs={{0,1},{1,2},{2,3},{3,0},{16,19},{17,16},{18,17},{19,18},{4,5},{5,6... | collective-permute-start | bytes 1179656 | tf_op jit(solution)/shard_map/ppermute | solution.py:225
  7.5 1.9 %collective-permute-start.1 = (bf16[3,64,1024]{2,1,0:T(8,128)(2,1)}, bf16[3,64,1024]{2,1,0:T(8,128)(2,1)S(1)}, u32[]{:S(2)}, u32[]{:S(2)}) collective-permute-start(bf16[3,64,1024]{2,1,0:T(8,128)(2,1)} %get-tuple-element.14), channel_id=1, source_target_pairs={{0,3},{1,0},{2,1},{3,2},{16,17},{17,18},{18,19},{19,16},{4,7},{5,4... | collective-permute-start | bytes 1179656 | tf_op jit(solution)/shard_map/ppermute | solution.py:226
  9.4 18.2 %all-to-all-start = ((bf16[64,8,128]{2,1,0:T(8,128)(2,1)}), bf16[64,8,128]{2,1,0:T(8,128)(2,1)S(1)}, u32[]{:S(2)}, u32[]{:S(2)}) async-start(bf16[64,8,128]{2,1,0:T(8,128)(2,1)} %bitcast.43), calls=%async_computation | async-start | bytes 262144 | tf_op jit(solution)/shard_map/all_to_all | solution.py:275
  27.7 0.0 copy-start.2
  27.7 0.0 copy-start
  27.7 0.0 copy-start.1
  27.7 0.6 copy-done.2
  28.4 0.0 copy-done
  28.4 0.0 copy-done.1
  28.4 0.3 shard_map.75
  28.7 0.0 collective-permute-done
  28.7 0.7 slice.26
  29.4 4.1 %collective-permute-start.2 = (bf16[2,64,1024]{2,1,0:T(8,128)(2,1)}, bf16[2,64,1024]{2,1,0:T(8,128)(2,1)}, u32[]{:S(2)}, u32[]{:S(2)}) collective-permute-start(bf16[2,64,1024]{2,1,0:T(8,128)(2,1)} %slice.26), channel_id=1, source_target_pairs={{0,1},{1,2},{2,3},{3,0},{16,19},{17,16},{18,17},{19,18},{4,5},{5,6... | collective-permute-start | bytes 786440 | tf_op jit(solution)/shard_map/ppermute | solution.py:227
  33.5 0.1 broadcast_in_dim.21
  33.7 0.0 copy-start.3
  33.7 0.0 collective-permute-done.1
  33.7 0.9 copy-done.3
  34.7 0.1 broadcast_in_dim.26
  34.8 8.2 %all-to-all-done = bf16[64,8,128]{2,1,0:T(8,128)(2,1)S(1)} async-done(((bf16[64,8,128]{2,1,0:T(8,128)(2,1)}), bf16[64,8,128]{2,1,0:T(8,128)(2,1)S(1)}, u32[]{:S(2)}, u32[]{:S(2)}) %all-to-all-start) | async-done | bytes 131104 | tf_op jit(solution)/shard_map/all_to_all | solution.py:275
  43.0 0.8 shard_map.74
  43.8 7.7 %all-to-all-start.1 = ((bf16[8,256,128]{2,1,0:T(8,128)(2,1)}), bf16[8,256,128]{2,1,0:T(8,128)(2,1)S(1)}, u32[]{:S(2)}, u32[]{:S(2)}) async-start(bf16[8,256,128]{2,1,0:T(8,128)(2,1)} %bitcast.10), calls=%async_computation.1 | async-start | bytes 1048576 | tf_op jit(solution)/shard_map/all_to_all | solution.py:286
  51.6 0.9 slice_dynamic-update-slice_fusion.1
  52.5 0.0 collective-permute-done.2
  52.5 1.0 bitcast_dynamic-update-slice_fusion.weights_ref
  53.5 7.4 %all-to-all-done.1 = bf16[8,256,128]{2,1,0:T(8,128)(2,1)S(1)} async-done(((bf16[8,256,128]{2,1,0:T(8,128)(2,1)}), bf16[8,256,128]{2,1,0:T(8,128)(2,1)S(1)}, u32[]{:S(2)}, u32[]{:S(2)}) %all-to-all-start.1) | async-done | bytes 524320 | tf_op jit(solution)/shard_map/all_to_all | solution.py:286
  60.9 0.4 shard_map.76.normed
  61.3 1.3 %shard_map.77 = bf16[4,256,256]{2,1,0:T(8,128)(2,1)} custom-call(bf16[256,1024]{1,0:T(8,128)(2,1)S(1)} %shard_map.76.normed, bf16[4,2,64,1024]{3,2,1,0:T(8,128)(2,1)S(1)} %bitcast_dynamic-update-slice_fusion.weights_ref), custom_call_target="tpu_custom_call" | custom-call | flops 268435456 | bytes 1048576 | tf_op jit(solution)/shard_map/pallas_call | solution.py:197
  62.6 3.5 %all-to-all-start.2 = ((bf16[4,256,256]{2,1,0:T(8,128)(2,1)}), bf16[4,256,256]{2,1,0:T(8,128)(2,1)S(1)}, u32[]{:S(2)}, u32[]{:S(2)}) async-start(bf16[4,256,256]{2,1,0:T(8,128)(2,1)} %shard_map.77), calls=%async_computation.2 | async-start | bytes 1048576 | tf_op jit(solution)/shard_map/all_to_all | solution.py:304
  66.1 2.2 %collective-permute-start.3 = (bf16[64,1024]{1,0:T(8,128)(2,1)S(1)}, bf16[64,1024]{1,0:T(8,128)(2,1)S(1)}, u32[]{:S(2)}, u32[]{:S(2)}) collective-permute-start(bf16[64,1024]{1,0:T(8,128)(2,1)S(1)} %get-tuple-element.17), channel_id=1, source_target_pairs={{0,3},{1,0},{2,1},{3,2},{16,17},{17,18},{18,19},{19,16},{4,7},{5,4... | collective-permute-start | bytes 393224 | tf_op jit(solution)/shard_map/ppermute | solution.py:228
  68.3 5.0 %collective-permute-done.3 = bf16[64,1024]{1,0:T(8,128)(2,1)S(1)} collective-permute-done((bf16[64,1024]{1,0:T(8,128)(2,1)S(1)}, bf16[64,1024]{1,0:T(8,128)(2,1)S(1)}, u32[]{:S(2)}, u32[]{:S(2)}) %collective-permute-start.3) | collective-permute-done | bytes 131104 | tf_op jit(solution)/shard_map/ppermute | solution.py:228
  73.3 2.0 %all-to-all-done.2.hidden_ref = bf16[4,256,256]{2,1,0:T(8,128)(2,1)S(1)} async-done(((bf16[4,256,256]{2,1,0:T(8,128)(2,1)}), bf16[4,256,256]{2,1,0:T(8,128)(2,1)S(1)}, u32[]{:S(2)}, u32[]{:S(2)}) %all-to-all-start.2) | async-done | bytes 524320 | tf_op jit(solution)/shard_map/all_to_all | solution.py:304
  75.3 0.4 shard_map.78
  75.7 24.1 %all_to_all.20 = bf16[128,4,128]{2,1,0:T(4,128)(2,1)S(1)} all-to-all(bf16[128,4,128]{2,1,0:T(4,128)(2,1)S(1)} %bitcast.36), channel_id=1, replica_groups=mesh['z'=16,'core'=2,'ty'=4,'tx'=4] {'z','core','tx'}, dimensions={0} | all-to-all | bytes 262144 | tf_op jit(solution)/shard_map/all_to_all | solution.py:314
  99.8 0.9 shard_map.79
  (6 shorter events, 0.1 us)
Async XLA Ops:
  2.3 26.4 %collective-permute-start = (bf16[3,64,1024]{2,1,0:T(8,128)(2,1)}, bf16[3,64,1024]{2,1,0:T(8,128)(2,1)S(1)}, u32[]{:S(2)}, u32[]{:S(2)}) collective-permute-start(bf16[3,64,1024]{2,1,0:T(8,128)(2,1)} %get-tuple-element.14), channel_id=1, source_target_pairs={{0,1},{1,2},{2,3},{3,0},{16,19},{17,16},{18,17},{19,18},{4,5},{5,6... | collective-permute-start | bytes 1179656 | tf_op jit(solution)/shard_map/ppermute | solution.py:225
  7.5 26.2 %collective-permute-start.1 = (bf16[3,64,1024]{2,1,0:T(8,128)(2,1)}, bf16[3,64,1024]{2,1,0:T(8,128)(2,1)S(1)}, u32[]{:S(2)}, u32[]{:S(2)}) collective-permute-start(bf16[3,64,1024]{2,1,0:T(8,128)(2,1)} %get-tuple-element.14), channel_id=1, source_target_pairs={{0,3},{1,0},{2,1},{3,2},{16,17},{17,18},{18,19},{19,16},{4,7},{5,4... | collective-permute-start | bytes 1179656 | tf_op jit(solution)/shard_map/ppermute | solution.py:226
  9.4 33.5 %all-to-all-start = ((bf16[64,8,128]{2,1,0:T(8,128)(2,1)}), bf16[64,8,128]{2,1,0:T(8,128)(2,1)S(1)}, u32[]{:S(2)}, u32[]{:S(2)}) async-start(bf16[64,8,128]{2,1,0:T(8,128)(2,1)} %bitcast.43), calls=%async_computation | async-start | bytes 262144 | tf_op jit(solution)/shard_map/all_to_all | solution.py:275
  27.7 0.7 copy-start.2
  27.7 0.7 copy-start
  27.7 0.7 copy-start.1
  29.4 23.1 %collective-permute-start.2 = (bf16[2,64,1024]{2,1,0:T(8,128)(2,1)}, bf16[2,64,1024]{2,1,0:T(8,128)(2,1)}, u32[]{:S(2)}, u32[]{:S(2)}) collective-permute-start(bf16[2,64,1024]{2,1,0:T(8,128)(2,1)} %slice.26), channel_id=1, source_target_pairs={{0,1},{1,2},{2,3},{3,0},{16,19},{17,16},{18,17},{19,18},{4,5},{5,6... | collective-permute-start | bytes 786440 | tf_op jit(solution)/shard_map/ppermute | solution.py:227
  33.7 1.0 copy-start.3
  43.8 17.1 %all-to-all-start.1 = ((bf16[8,256,128]{2,1,0:T(8,128)(2,1)}), bf16[8,256,128]{2,1,0:T(8,128)(2,1)S(1)}, u32[]{:S(2)}, u32[]{:S(2)}) async-start(bf16[8,256,128]{2,1,0:T(8,128)(2,1)} %bitcast.10), calls=%async_computation.1 | async-start | bytes 1048576 | tf_op jit(solution)/shard_map/all_to_all | solution.py:286
  62.6 12.7 %all-to-all-start.2 = ((bf16[4,256,256]{2,1,0:T(8,128)(2,1)}), bf16[4,256,256]{2,1,0:T(8,128)(2,1)S(1)}, u32[]{:S(2)}, u32[]{:S(2)}) async-start(bf16[4,256,256]{2,1,0:T(8,128)(2,1)} %shard_map.77), calls=%async_computation.2 | async-start | bytes 1048576 | tf_op jit(solution)/shard_map/all_to_all | solution.py:304
  66.1 7.2 %collective-permute-start.3 = (bf16[64,1024]{1,0:T(8,128)(2,1)S(1)}, bf16[64,1024]{1,0:T(8,128)(2,1)S(1)}, u32[]{:S(2)}, u32[]{:S(2)}) collective-permute-start(bf16[64,1024]{1,0:T(8,128)(2,1)S(1)} %get-tuple-element.17), channel_id=1, source_target_pairs={{0,3},{1,0},{2,1},{3,2},{16,17},{17,18},{18,19},{19,16},{4,7},{5,4... | collective-permute-start | bytes 393224 | tf_op jit(solution)/shard_map/ppermute | solution.py:228
